TPU v7x, 32 devices: a whole 2x2x4 slice. The times are simulated.
32 devices in a mesh: ep: 8 (over z, core), tp: 4 (over y, x).
Axes of the slice: x: 2, y: 2, z: 4, core: 2. Of those that a mesh axis runs over, the one named last changes fastest.
Arguments:
- query_vectors: bfloat16 [4096, 4096], P('ep', 'tp'), may hold values from -6 to 6
- key_vectors: bfloat16 [4096, 2048], P('ep', 'tp'), may hold values from -6 to 6
- value_vectors: bfloat16 [4096, 2048], P('ep', 'tp'), may hold values from -64 to 64
- query_gain: float32 [128], replicated, may hold values from 0.1 to 1.9
- key_gain: float32 [128], replicated, may hold values from 0.1 to 1.9
- sink_logits: float32 [32], P('tp'), may hold values from 3 to 7
- moe_rows: bfloat16 [1280, 4096], P('ep', 'tp'), may hold values from -6 to 6
- norm_gain: float32 [4096], replicated, may hold values from 0.1 to 1.9
- expert_ids: int32 [1280, 4], P('ep'), may hold values from 0 to 7, all different within a row; in each aligned block of 160 rows (0 to 159, 160 to 319, ...) at most 120 rows name the same one
- route_weights: float32 [1280, 4], P('ep'), may hold values from 0.25 to 2.5
- expert_gate: bfloat16 [8, 4096, 2048], P('ep', None, 'tp'), may hold values from -0.09375 to 0.09375
- expert_up: bfloat16 [8, 4096, 2048], P('ep', None, 'tp'), may hold values from -0.09375 to 0.09375
- expert_down: bfloat16 [8, 2048, 4096], P('ep', None, 'tp'), may hold values from -0.125 to 0.125
- shared_gate: bfloat16 [4096, 512], P(None, 'tp'), may hold values from -0.09375 to 0.09375
- shared_up: bfloat16 [4096, 512], P(None, 'tp'), may hold values from -0.09375 to 0.09375
- shared_down: bfloat16 [512, 4096], P(None, 'tp'), may hold values from -0.25 to 0.25
Outputs:
- attended: bfloat16 [4096, 4096], P('ep', 'tp')
- moe_out: bfloat16 [1280, 4096], P('ep', 'tp')
Inputs may be any that keep to these rules, and one draw needn't show every extreme that they name: `expert_ids`: each row names 4 different experts. Within the rows of one index of ep (aligned blocks of 160 rows), no expert is named by more than 120 rows, and in some block one expert is named by exactly 120.
All inputs are finite; a program needn't handle non-finite values.
Results may differ from a plain program's by a relative error of at most 0.0071.
Values may be sent and summed in bfloat16 or wider, within the bound.
A program may use at most 128 MiB of HBM per device.

v0:
```python
import functools

import jax
import jax.numpy as jnp
from jax import lax
from jax.experimental import pallas as pl
from jax.experimental.pallas import tpu as pltpu
from jax.sharding import PartitionSpec as P

HEAD_DIM = 128
WINDOW = 128
GRID_W = 64
D = 4096
TOP_K = 4


epsilon = 1e-06
rotary_base = 10000.0


def padded_2(block, sides, width):
    for axis, dim in sides:
        count = lax.axis_size(axis)
        forward = [(i, i + 1) for i in range(count - 1)]
        backward = [(target, source) for source, target in forward]
        low = lax.ppermute(
            lax.slice_in_dim(block, block.shape[dim] - width, None, axis=dim), axis, forward
        )
        high = lax.ppermute(lax.slice_in_dim(block, 0, width, axis=dim), axis, backward)
        block = jnp.concatenate([low, block, high], axis=dim)
    return block


def half_turn(halves):
    leading, trailing = jnp.split(halves, 2, axis=-1)
    return jnp.concatenate([-trailing, leading], axis=-1)


def rotate_heads(vectors, head_gain, positions):
    floats = vectors.astype(jnp.float32)
    normed = (
        floats * lax.rsqrt(jnp.mean(floats * floats, axis=-1, keepdims=True) + epsilon) * head_gain
    )
    quarter = HEAD_DIM // 4
    freq_index = jnp.arange(quarter, dtype=jnp.int32).astype(jnp.float32)
    inverse = rotary_base ** (-4.0 * freq_index / HEAD_DIM)
    grid_row = (positions // GRID_W).astype(jnp.float32)[:, None] * inverse
    grid_col = (positions % GRID_W).astype(jnp.float32)[:, None] * inverse
    angles = jnp.concatenate([grid_row, grid_row, grid_col, grid_col], axis=-1)[:, None, :]
    row_half, col_half = jnp.split(normed, 2, axis=-1)
    turned = jnp.concatenate([half_turn(row_half), half_turn(col_half)], axis=-1)
    return (normed * jnp.cos(angles) + turned * jnp.sin(angles)).astype(jnp.bfloat16)


def attend_window(query_vectors, key_vectors, value_vectors, query_gain, key_gain, sink_logits):
    length = query_vectors.shape[0]
    heads_here = sink_logits.shape[0]
    kv_here = key_vectors.shape[1] // HEAD_DIM
    grouping = heads_here // kv_here
    shard_start = lax.axis_index("ep") * length
    positions = shard_start + jnp.arange(length, dtype=jnp.int32)
    queries = rotate_heads(
        query_vectors.reshape(length, heads_here, HEAD_DIM), query_gain, positions
    )
    turned_keys = rotate_heads(key_vectors.reshape(length, kv_here, HEAD_DIM), key_gain, positions)
    turned_keys = turned_keys.reshape(length, kv_here * HEAD_DIM)
    padded = padded_2(jnp.stack([turned_keys, value_vectors]), (("ep", 1),), WINDOW)
    extent = length + 2 * WINDOW
    near_keys = padded[0].reshape(extent, kv_here, HEAD_DIM)
    near_values = padded[1].reshape(extent, kv_here, HEAD_DIM)
    key_pos = shard_start - WINDOW + jnp.arange(extent, dtype=jnp.int32)
    inside = (
        (jnp.abs(positions[:, None] - key_pos[None, :]) <= WINDOW)
        & (key_pos >= 0)[None, :]
        & (key_pos < lax.axis_size("ep") * length)[None, :]
    )
    scores = jnp.einsum(
        "qhgd,khd->hgqk",
        queries.reshape(length, kv_here, grouping, HEAD_DIM),
        near_keys,
        preferred_element_type=jnp.float32,
    ) * HEAD_DIM ** (-0.5)
    raised = jnp.where(inside, jnp.exp(scores), 0.0)
    denominator = jnp.exp(sink_logits).reshape(kv_here, grouping)[:, :, None] + jnp.sum(
        raised, axis=-1
    )
    weights = (raised / denominator[..., None]).astype(jnp.bfloat16)
    mixed = jnp.einsum("hgqk,khd->qhgd", weights, near_values, preferred_element_type=jnp.float32)
    return mixed.astype(jnp.bfloat16).reshape(length, heads_here * HEAD_DIM)


def project(block_rows, gain_piece, gate_rows, up_rows):
    floats = block_rows.astype(jnp.float32)
    weighted = (floats * gain_piece).astype(jnp.bfloat16)
    gate_sum = jnp.dot(weighted, gate_rows, preferred_element_type=jnp.float32)
    up_sum = jnp.dot(weighted, up_rows, preferred_element_type=jnp.float32)
    return (gate_sum, up_sum, jnp.sum(floats * floats, axis=1))


def activate(gate_sum, up_sum, squares):
    factor = lax.rsqrt(squares / D + epsilon)[:, None]
    return (jax.nn.silu(gate_sum * factor) * (up_sum * factor)).astype(jnp.bfloat16)


def shards(
    query_vectors,
    key_vectors,
    value_vectors,
    query_gain,
    key_gain,
    sink_logits,
    moe_rows,
    norm_gain,
    expert_ids,
    route_weights,
    expert_gate,
    expert_up,
    expert_down,
    shared_gate,
    shared_up,
    shared_down,
):
    attended = attend_window(
        query_vectors, key_vectors, value_vectors, query_gain, key_gain, sink_logits
    )
    ep_size = lax.axis_size("ep")
    tokens_here, width_here = moe_rows.shape
    capacity = max(2, 3 * tokens_here * TOP_K // (2 * ep_size))
    slots_all = ep_size * capacity
    flat_ids = expert_ids.reshape(-1)
    onehot = (flat_ids[:, None] == jnp.arange(ep_size, dtype=jnp.int32)[None, :]).astype(jnp.int32)
    slot_index = jnp.sum((jnp.cumsum(onehot, axis=0) - onehot) * onehot, axis=1)
    target = flat_ids * capacity + slot_index
    matches = target[None, :] == jnp.arange(slots_all, dtype=jnp.int32)[:, None]
    present = jnp.any(matches, axis=1)
    owner_row = jnp.arange(tokens_here * TOP_K, dtype=jnp.int32) // TOP_K
    source_row = jnp.sum(jnp.where(matches, owner_row[None, :], 0), axis=1)
    local_gate = expert_gate[0]
    local_up = expert_up[0]
    local_down = expert_down[0]
    units_here = local_gate.shape[1]
    shared_units = shared_gate.shape[1]
    outgoing = jnp.where(
        present[:, None], jnp.take(moe_rows, source_row, axis=0), jnp.zeros((), jnp.bfloat16)
    )
    arrived = lax.all_to_all(
        outgoing.reshape(ep_size, capacity, width_here),
        "ep",
        split_axis=0,
        concat_axis=0,
        tiled=True,
    )
    arrived = arrived.reshape(slots_all, width_here)
    routed = project(
        lax.all_gather(arrived, "tp", axis=1, tiled=True), norm_gain, local_gate, local_up
    )
    shared = project(
        lax.all_gather(moe_rows, "tp", axis=1, tiled=True), norm_gain, shared_gate, shared_up
    )
    gate_sum, up_sum, squares, shared_gsum, shared_usum, own_squares = tuple(
        (new_term for new_term in routed + shared)
    )
    hidden = activate(gate_sum, up_sum, squares)
    shared_hidden = activate(shared_gsum, shared_usum, own_squares)
    packing = units_here // shared_units
    stacked = jnp.concatenate(
        [hidden, shared_hidden.reshape(tokens_here // packing, units_here)], axis=0
    )
    columns = local_down.shape[1]
    portion = lax.all_gather(stacked, "tp", axis=1, tiled=True)
    shards_in = portion.shape[1] // units_here
    routed = jnp.dot(portion[:slots_all], local_down, preferred_element_type=jnp.float32)
    shared_piece = portion[slots_all:].reshape(
        tokens_here // packing, shards_in, packing, shared_units
    )
    shared_piece = shared_piece.transpose(0, 2, 1, 3).reshape(tokens_here, shards_in * shared_units)
    shared = jnp.dot(shared_piece, shared_down, preferred_element_type=jnp.float32)
    returned = lax.all_to_all(
        routed.astype(jnp.bfloat16).reshape(ep_size, capacity, columns),
        "ep",
        split_axis=0,
        concat_axis=0,
        tiled=True,
    )
    returned = returned.reshape(slots_all, columns)
    picked = jnp.take(returned, target, axis=0).reshape(tokens_here, TOP_K, columns)
    combined = shared + jnp.sum(route_weights[:, :, None] * picked.astype(jnp.float32), axis=1)
    return (attended, combined.astype(jnp.bfloat16))


F32 = jnp.float32
BF16 = jnp.bfloat16
MESH = pl.DeviceIdType.MESH
LANES = 128


def moe_kernel(
    sizes,
    q_hbm,
    k_hbm,
    v_hbm,
    cos_ref,
    sin_ref,
    qgain_ref,
    kgain_ref,
    sink_ref,
    x_hbm,
    gain_ref,
    wt_hbm,
    gate_hbm,
    up_hbm,
    down_hbm,
    sgate_hbm,
    sup_hbm,
    sdown_hbm,
    att_ref,
    out_ref,
    xbuf,
    gate,
    up,
    down,
    sgate,
    sup,
    sdown,
    qbuf,
    kbuf,
    vbuf,
    wbuf,
    scaled,
    factor,
    hid,
    hbuf,
    shbuf,
    pbuf,
    prx,
    qtx,
    qrx,
    local_sem,
    zs,
    zr,
    xs,
    xr,
    ys,
    yr,
    dxs,
    dxr,
    dys,
    dyr,
    ps,
    pr,
    hxs,
    hxr,
    hys,
    hyr,
    gxs,
    gxr,
    gys,
    gyr,
    ss,
    sr,
    ws,
    wr,
    ks,
    kr,
    pps,
    ppr,
    qqs,
    qqr,
):
    ep, tp, nz, tok, width, cap, tok_a, kv_heads, group, units, columns, sunits = sizes
    e = lax.axis_index("ep")
    t = lax.axis_index("tp")
    z, c = e // 2, e % 2
    other = 1 - c
    partner = z * 2 + other
    tx, ty = t % 2, t // 2
    xn = ty * 2 + (1 - tx)
    yn = (1 - ty) * 2 + tx
    dn = (1 - ty) * 2 + (1 - tx)
    half = tok // 2
    slots = 2 * cap
    hcut = (slots // 2 + 15) // 16 * 16
    row_c = pl.multiple_of(c * tok, 16)
    row_o = pl.multiple_of(other * tok, 16)

    def rc(src, dst, s_sem, r_sem, dev):
        return pltpu.make_async_remote_copy(
            src_ref=src,
            dst_ref=dst,
            send_sem=s_sem,
            recv_sem=r_sem,
            device_id=dev,
            device_id_type=MESH,
        )

    unit0 = xbuf.at[z, t, pl.ds(row_c, tok), :]
    loads = [
        (x_hbm, unit0),
        (wt_hbm, wbuf.at[e]),
        (k_hbm, kbuf.at[pl.ds(WINDOW, tok_a), :]),
        (v_hbm, vbuf.at[pl.ds(WINDOW, tok_a), :]),
        (q_hbm, qbuf),
        (gate_hbm.at[0], gate),
        (up_hbm.at[0], up),
        (sgate_hbm, sgate),
        (sup_hbm, sup),
        (down_hbm.at[0], down),
        (sdown_hbm, sdown),
    ]
    copies = [
        pltpu.make_async_copy(a, b, local_sem.at[i]) for i, (a, b) in enumerate(loads)
    ]
    for cp in copies:
        cp.start()

    barrier = pltpu.get_barrier_semaphore()
    for d in range(1, ep):
        pl.semaphore_signal(barrier, inc=1, device_id=((e + d) % ep, t), device_id_type=MESH)
    for d in range(1, tp):
        pl.semaphore_signal(barrier, inc=1, device_id=(e, (t + d) % tp), device_id_type=MESH)
    pl.semaphore_wait(barrier, ep + tp - 2)

    def unit(zi, ti, row, first=0, count=tok):
        return xbuf.at[zi, ti, pl.ds(row + first, count), :]

    def z_copy(d):
        zi = (z + d) % nz
        return rc(unit0, unit0, zs.at[d], zr.at[z], (zi * 2 + c, t))

    def z_landed(zi):
        u = unit(zi, t, row_c)
        return rc(u, u, zs.at[0], zr.at[zi], (e, xn))

    def x_copy(zi):
        u = unit(zi, t, row_c)
        return rc(u, u, xs.at[zi], xr.at[zi], (e, xn))

    def y_copy(zi):
        u = unit(zi, t, row_c)
        return rc(u, u, ys.at[zi], yr.at[zi], (e, yn))

    def x_landed(zi):
        u = unit(zi, xn, row_c)
        return rc(u, u, xs.at[zi], xr.at[zi], (e, xn))

    def y_landed(zi):
        u = unit(zi, yn, row_c)
        return rc(u, u, ys.at[zi], yr.at[zi], (e, yn))

    def dy_copy(zi):
        u = unit(zi, xn, row_c, 0, half)
        return rc(u, u, dys.at[zi], dyr.at[zi], (e, yn))

    def dx_copy(zi):
        u = unit(zi, yn, row_c, half, half)
        return rc(u, u, dxs.at[zi], dxr.at[zi], (e, xn))

    def dy_landed(zi):
        u = unit(zi, dn, row_c, 0, half)
        return rc(u, u, dys.at[zi], dyr.at[zi], (e, yn))

    def dx_landed(zi):
        u = unit(zi, dn, row_c, half, half)
        return rc(u, u, dxs.at[zi], dxr.at[zi], (e, xn))

    def p_copy(zi, ti):
        u = unit(zi, ti, row_c)
        return rc(u, u, ps.at[zi, ti], pr.at[zi, ti], (partner, t))

    def p_landed(zi, ti):
        u = unit(zi, ti, row_o)
        return rc(u, u, ps.at[zi, ti], pr.at[zi, ti], (partner, t))

    def hx_copy(zi):
        u = hbuf.at[zi, t]
        return rc(u, u, hxs.at[zi], hxr.at[zi], (e, xn))

    def hy_copy(zi):
        u = hbuf.at[zi, t]
        return rc(u, u, hys.at[zi], hyr.at[zi], (e, yn))

    def hx_landed(zi):
        u = hbuf.at[zi, xn]
        return rc(u, u, hxs.at[zi], hxr.at[zi], (e, xn))

    def hy_landed(zi):
        u = hbuf.at[zi, yn]
        return rc(u, u, hys.at[zi], hyr.at[zi], (e, yn))

    def gy_copy(zi):
        u = hbuf.at[zi, xn, pl.ds(0, hcut), :]
        return rc(u, u, gys.at[zi], gyr.at[zi], (e, yn))

    def gx_copy(zi):
        u = hbuf.at[zi, yn, pl.ds(hcut, slots - hcut), :]
        return rc(u, u, gxs.at[zi], gxr.at[zi], (e, xn))

    def gy_landed(zi):
        u = hbuf.at[zi, dn, pl.ds(0, hcut), :]
        return rc(u, u, gys.at[zi], gyr.at[zi], (e, yn))

    def gx_landed(zi):
        u = hbuf.at[zi, dn, pl.ds(hcut, slots - hcut), :]
        return rc(u, u, gxs.at[zi], gxr.at[zi], (e, xn))

    def s_copy(d):
        u = shbuf.at[t]
        return rc(u, u, ss.at[d], sr.at[t], (e, (t + d) % tp))

    def s_landed(ti):
        u = shbuf.at[ti]
        return rc(u, u, ss.at[0], sr.at[ti], (e, xn))

    def w_copy(d):
        u = wbuf.at[e]
        return rc(u, u, ws.at[d], wr.at[e], ((e + d) % ep, t))

    def w_landed(ei):
        u = wbuf.at[ei]
        return rc(u, u, ws.at[0], wr.at[ei], (partner, t))

    after, before = (e + 1) % ep, (e + ep - 1) % ep
    tail = pl.ds(tok_a, WINDOW)
    first = pl.ds(WINDOW, WINDOW)
    low = pl.ds(0, WINDOW)
    high = pl.ds(WINDOW + tok_a, WINDOW)
    halos = [
        rc(kbuf.at[tail, :], kbuf.at[low, :], ks.at[0], kr.at[0], (after, t)),
        rc(kbuf.at[first, :], kbuf.at[high, :], ks.at[1], kr.at[1], (before, t)),
        rc(vbuf.at[tail, :], vbuf.at[low, :], ks.at[2], kr.at[2], (after, t)),
        rc(vbuf.at[first, :], vbuf.at[high, :], ks.at[3], kr.at[3], (before, t)),
    ]

    def pp_copy(zi):
        return rc(pbuf.at[zi, other], prx.at[zi], pps.at[zi], ppr.at[zi], (partner, t))

    def qq_copy(zi):
        return rc(qtx.at[zi], qrx.at[z], qqs.at[zi], qqr.at[z], (zi * 2 + c, t))

    def qq_landed(zi):
        return rc(qrx.at[zi], qrx.at[zi], qqs.at[zi], qqr.at[zi], (partner, t))

    copies[0].wait()
    x_copy(z).start()
    y_copy(z).start()
    for d in range(1, nz):
        z_copy(d).start()
    p_copy(z, t).start()
    copies[1].wait()
    for d in range(1, ep):
        w_copy(d).start()
    copies[2].wait()
    copies[3].wait()
    for h in halos:
        h.start()
    copies[4].wait()

    lane = lax.broadcasted_iota(jnp.int32, (WINDOW, LANES), 1)
    leading = (lane % (HEAD_DIM // 2)) < HEAD_DIM // 4

    def turn(block, head_gain, table_rows):
        v = block.astype(F32)
        v = v * lax.rsqrt(jnp.mean(v * v, axis=-1, keepdims=True) + epsilon) * head_gain
        swapped = jnp.where(
            leading,
            pltpu.roll(v, HEAD_DIM - HEAD_DIM // 4, 1),
            pltpu.roll(v, HEAD_DIM // 4, 1),
        )
        return (v * cos_ref[table_rows, :] + swapped * sin_ref[table_rows, :]).astype(BF16)

    heads = kv_heads * group

    def turn_q(i, carry):
        rows = pl.ds(pl.multiple_of(i * WINDOW, WINDOW), WINDOW)
        table = pl.ds(pl.multiple_of((i + 1) * WINDOW, WINDOW), WINDOW)
        for h in range(heads):
            cols = slice(h * HEAD_DIM, (h + 1) * HEAD_DIM)
            qbuf[rows, cols] = turn(qbuf[rows, cols], qgain_ref[...], table)
        return carry

    nq = tok_a // WINDOW
    lax.fori_loop(0, nq, turn_q, 0)

    def forward_z(zi):
        z_landed(zi).wait_recv()
        x_copy(zi).start()
        y_copy(zi).start()
        p_copy(zi, t).start()

    forward_z((z + 1) % nz)

    for h in halos:
        h.wait()

    def turn_k(i, carry):
        rows = pl.ds(pl.multiple_of(i * WINDOW, WINDOW), WINDOW)
        for h in range(kv_heads):
            cols = slice(h * HEAD_DIM, (h + 1) * HEAD_DIM)
            kbuf[rows, cols] = turn(kbuf[rows, cols], kgain_ref[...], rows)
        return carry

    lax.fori_loop(0, nq + 2, turn_k, 0)
    for d in range(1, ep):
        w_landed((e + d) % ep).wait_recv()
    for cp in copies[5:]:
        cp.wait()

    span = 3 * WINDOW

    def attend(i, carry):
        qb, kh = i // kv_heads, i % kv_heads
        rows = pl.ds(pl.multiple_of(qb * WINDOW, WINDOW), WINDOW)
        keys = pl.ds(pl.multiple_of(qb * WINDOW, WINDOW), span)
        kcols = pl.ds(pl.multiple_of(kh * HEAD_DIM, HEAD_DIM), HEAD_DIM)
        near = lax.broadcasted_iota(jnp.int32, (WINDOW, span), 1)
        mine = lax.broadcasted_iota(jnp.int32, (WINDOW, span), 0)
        pos = e * tok_a + (qb - 1) * WINDOW + near
        inside = (
            (near - mine >= 0) & (near - mine <= 2 * WINDOW) & (pos >= 0) & (pos < ep * tok_a)
        )
        kk = kbuf[keys, kcols]
        vv = vbuf[keys, kcols]
        for g in range(group):
            qcols = pl.ds(
                pl.multiple_of((kh * group + g) * HEAD_DIM, HEAD_DIM), HEAD_DIM
            )
            scores = lax.dot_general(
                qbuf[rows, qcols], kk, (((1,), (1,)), ((), ())), preferred_element_type=F32
            )
            raised = jnp.where(inside, jnp.exp(scores * HEAD_DIM ** (-0.5)), 0.0)
            sink = jnp.exp(sink_ref[kh * group + g])
            total = jnp.sum(raised, axis=-1, keepdims=True) + sink[0:1, 0:1]
            weights = (raised * (1.0 / total)).astype(BF16)
            att_ref[rows, qcols] = jnp.dot(weights, vv, preferred_element_type=F32).astype(BF16)
        return carry

    upper = (
        lax.broadcasted_iota(jnp.int32, (tok, tok), 0)
        < lax.broadcasted_iota(jnp.int32, (tok, tok), 1)
    ).astype(F32)

    def picks(block):
        weight = wbuf[block, pl.ds(e, 1), :][:, :tok]
        named = jnp.where(weight > 0.0, 1.0, 0.0)
        rank = jnp.dot(
            jnp.broadcast_to(named, (16, tok)).astype(BF16),
            upper.astype(BF16),
            preferred_element_type=F32,
        )[0:1, :]
        slot = lax.broadcasted_iota(jnp.int32, (cap, tok), 0).astype(F32)
        hot = jnp.where((slot == rank) & (named > 0.0), 1.0, 0.0)
        return hot, jnp.sum(hot * weight, axis=1, keepdims=True)

    chunk = 32

    def silu_pair(g, u, f):
        g = g * f
        return g / (1.0 + jnp.exp(-g)) * (u * f)

    tile = min(256, units)

    def project_pair(zi):
        def scale(i, carry):
            rows = pl.ds(pl.multiple_of(i * chunk, chunk), chunk)
            squares = jnp.zeros((chunk, 1), F32)
            for ti in range(tp):
                v = xbuf[zi, ti, rows, :].astype(F32)
                squares += jnp.sum(v * v, axis=1, keepdims=True)
                cols = slice(ti * width, (ti + 1) * width)
                scaled[rows, cols] = (v * gain_ref[:, cols]).astype(BF16)
            f = lax.rsqrt(squares / (tp * width) + epsilon)
            factor[rows, :] = jnp.broadcast_to(f, (chunk, LANES))
            return carry

        lax.fori_loop(0, 2 * tok // chunk, scale, 0)

        def columns_of(n, carry):
            cols = pl.ds(pl.multiple_of(n * tile, tile), tile)
            g = jnp.dot(scaled[...], gate[:, cols], preferred_element_type=F32)
            u = jnp.dot(scaled[...], up[:, cols], preferred_element_type=F32)
            hid[:, cols] = silu_pair(g, u, factor[:, 0:1]).astype(BF16)
            return carry

        lax.fori_loop(0, units // tile, columns_of, 0)
        parts = []
        for ci in range(2):
            hot, _ = picks(zi * 2 + ci)
            parts.append(
                jnp.dot(
                    hot.astype(BF16),
                    hid[ci * tok : (ci + 1) * tok, :],
                    preferred_element_type=F32,
                )
            )
        hbuf[zi, t] = jnp.concatenate(parts, axis=0).astype(BF16)

    def shared_up():
        rows = pl.ds(row_c, tok)
        g = jnp.dot(scaled[rows, :], sgate[...], preferred_element_type=F32)
        u = jnp.dot(scaled[rows, :], sup[...], preferred_element_type=F32)
        shbuf[t] = silu_pair(g, u, factor[rows, 0:1]).astype(BF16)

    ctile = min(256, columns)

    def down_pair(zi):
        picked = [picks(zi * 2 + ci) for ci in range(2)]
        slot_weight = jnp.concatenate([p[1] for p in picked], axis=0)

        def columns_of(n, carry):
            cols = pl.ds(pl.multiple_of(n * ctile, ctile), ctile)
            acc = jnp.zeros((slots, ctile), F32)
            for ti in range(tp):
                acc += jnp.dot(
                    hbuf[zi, ti],
                    down[ti * units : (ti + 1) * units, cols],
                    preferred_element_type=F32,
                )
            weighted = acc.astype(BF16).astype(F32) * slot_weight
            for ci in range(2):
                spread = lax.dot_general(
                    picked[ci][0].astype(BF16),
                    weighted[ci * cap : (ci + 1) * cap, :].astype(BF16),
                    (((0,), (0,)), ((), ())),
                    preferred_element_type=F32,
                )
                pbuf[zi, ci, :, cols] = spread.astype(BF16)
            return carry

        lax.fori_loop(0, columns // ctile, columns_of, 0)

    per_step = nq * kv_heads // nz

    def step(s, carry):
        @pl.when(s < nz)
        def _():
            lax.fori_loop(s * per_step, (s + 1) * per_step, attend, 0)
            zi = (z + s) % nz
            x_landed(zi).wait_recv()
            dy_copy(zi).start()
            p_copy(zi, xn).start()
            y_landed(zi).wait_recv()
            dx_copy(zi).start()
            p_copy(zi, yn).start()

            @pl.when(s + 2 < nz)
            def _():
                forward_z((z + s + 2) % nz)

            dy_landed(zi).wait_recv()
            dx_landed(zi).wait_recv()
            p_copy(zi, dn).start()
            for ti in range(tp):
                p_landed(zi, ti).wait_recv()
            project_pair(zi)
            hx_copy(zi).start()
            hy_copy(zi).start()

            @pl.when(s == 0)
            def _():
                shared_up()
                for d in range(1, tp):
                    s_copy(d).start()

        @pl.when((s >= 1) & (s < nz + 1))
        def _():
            zi = (z + s - 1) % nz
            hx_landed(zi).wait_recv()
            gy_copy(zi).start()
            hy_landed(zi).wait_recv()
            gx_copy(zi).start()

        @pl.when((s >= 2) & (s < nz + 2))
        def _():
            zi = (z + s - 2) % nz
            gy_landed(zi).wait_recv()
            gx_landed(zi).wait_recv()
            down_pair(zi)
            pp_copy(zi).start()
            pp_copy(zi).wait_recv()
            qtx[zi] = (pbuf[zi, c].astype(F32) + prx[zi].astype(F32)).astype(BF16)

            @pl.when(s > 2)
            def _():
                qq_copy(zi).start()

        return carry

    lax.fori_loop(0, nz + 2, step, 0)

    for d in range(1, tp):
        s_landed((t + d) % tp).wait_recv()
    for d in range(1, nz):
        qq_landed((z + d) % nz).wait_recv()
    for n in range(columns // ctile):
        cols = slice(n * ctile, (n + 1) * ctile)
        acc = qtx[z, :, cols].astype(F32)
        for d in range(1, nz):
            acc += qrx[(z + d) % nz, :, cols].astype(F32)
        for ti in range(tp):
            acc += jnp.dot(
                shbuf[ti],
                sdown[ti * sunits : (ti + 1) * sunits, cols],
                preferred_element_type=F32,
            )
        out_ref[:, cols] = acc.astype(BF16)

    for d in range(1, nz):
        z_copy(d).wait_send()
        qq_copy((z + d) % nz).wait_send()
    for d in range(1, tp):
        s_copy(d).wait_send()
    for d in range(1, ep):
        w_copy(d).wait_send()

    def drain(zi, carry):
        for kind in (x_copy, y_copy, dx_copy, dy_copy, hx_copy, hy_copy, gx_copy, gy_copy, pp_copy):
            kind(zi).wait_send()
        for ti in range(tp):
            p_copy(zi, ti).wait_send()
        return carry

    lax.fori_loop(0, nz, drain, 0)


def fast_shards(
    query_vectors,
    key_vectors,
    value_vectors,
    query_gain,
    key_gain,
    sink_logits,
    moe_rows,
    norm_gain,
    expert_ids,
    route_weights,
    expert_gate,
    expert_up,
    expert_down,
    shared_gate,
    shared_up,
    shared_down,
):
    ep, tp = lax.axis_size("ep"), lax.axis_size("tp")
    nz = ep // 2
    tok, width = moe_rows.shape
    cap = max(2, 3 * tok * TOP_K // (2 * ep))
    tok_a = query_vectors.shape[0]
    heads = sink_logits.shape[0]
    kv_heads = key_vectors.shape[1] // HEAD_DIM
    group = heads // kv_heads
    units = expert_gate.shape[2]
    columns = expert_down.shape[2]
    sunits = shared_gate.shape[1]
    sizes = (ep, tp, nz, tok, width, cap, tok_a, kv_heads, group, units, columns, sunits)
    full = tp * width

    extent = tok_a + 2 * WINDOW
    first_row = (lax.axis_index("ep") * tok_a - WINDOW) // GRID_W
    grid_rows = extent // GRID_W
    quarter = HEAD_DIM // 4
    inverse = rotary_base ** (-4.0 * jnp.arange(quarter, dtype=jnp.int32).astype(F32) / HEAD_DIM)
    row_ids = first_row + jnp.arange(grid_rows, dtype=jnp.int32)
    grid_row = row_ids.astype(F32)[:, None] * inverse
    grid_col = jnp.arange(GRID_W, dtype=jnp.int32).astype(F32)[:, None] * inverse

    def by_row(a):
        return jnp.broadcast_to(a[:, None, :], (grid_rows, GRID_W, quarter)).reshape(extent, quarter)

    def by_col(a):
        return jnp.broadcast_to(a[None], (grid_rows, GRID_W, quarter)).reshape(extent, quarter)

    cr, sr = by_row(jnp.cos(grid_row)), by_row(jnp.sin(grid_row))
    cc, sc = by_col(jnp.cos(grid_col)), by_col(jnp.sin(grid_col))
    cos = jnp.concatenate([cr, cr, cc, cc], axis=-1)
    sin = jnp.concatenate([-sr, sr, -sc, sc], axis=-1)

    experts = jnp.arange(ep, dtype=jnp.int32)
    table = jnp.sum(
        jnp.where(expert_ids.T[None, :, :] == experts[:, None, None], route_weights.T[None], 0.0),
        axis=1,
    )
    padded_tok = (tok + LANES - 1) // LANES * LANES
    table = jnp.pad(table, ((0, 0), (0, padded_tok - tok)))
    sinks = jnp.broadcast_to(sink_logits[:, None, None], (heads, 8, LANES))

    vm = pl.BlockSpec(memory_space=pltpu.VMEM)
    hb = pl.BlockSpec(memory_space=pl.ANY)
    dma = pltpu.SemaphoreType.DMA
    slots = 2 * cap
    zz = [dma((nz,))] * 2
    return pl.pallas_call(
        functools.partial(moe_kernel, sizes),
        out_shape=(
            jax.ShapeDtypeStruct((tok_a, heads * HEAD_DIM), BF16),
            jax.ShapeDtypeStruct((tok, columns), BF16),
        ),
        in_specs=[hb, hb, hb, vm, vm, vm, vm, vm, hb, vm, hb, hb, hb, hb, hb, hb, hb],
        out_specs=(vm, vm),
        scratch_shapes=[
            pltpu.VMEM((nz, tp, 2 * tok, width), BF16),
            pltpu.VMEM((full, units), BF16),
            pltpu.VMEM((full, units), BF16),
            pltpu.VMEM((tp * units, columns), BF16),
            pltpu.VMEM((full, sunits), BF16),
            pltpu.VMEM((full, sunits), BF16),
            pltpu.VMEM((tp * sunits, columns), BF16),
            pltpu.VMEM((tok_a, heads * HEAD_DIM), BF16),
            pltpu.VMEM((extent, kv_heads * HEAD_DIM), BF16),
            pltpu.VMEM((extent, kv_heads * HEAD_DIM), BF16),
            pltpu.VMEM((ep, ep, padded_tok), F32),
            pltpu.VMEM((2 * tok, full), BF16),
            pltpu.VMEM((2 * tok, LANES), F32),
            pltpu.VMEM((2 * tok, units), BF16),
            pltpu.VMEM((nz, tp, slots, units), BF16),
            pltpu.VMEM((tp, tok, sunits), BF16),
            pltpu.VMEM((nz, 2, tok, columns), BF16),
            pltpu.VMEM((nz, tok, columns), BF16),
            pltpu.VMEM((nz, tok, columns), BF16),
            pltpu.VMEM((nz, tok, columns), BF16),
            dma((11,)),
        ]
        + zz * 5
        + [dma((nz, tp))] * 2
        + zz * 4
        + [dma((tp,))] * 2
        + [dma((ep,))] * 2
        + [dma((4,))] * 2
        + zz * 2,
        compiler_params=pltpu.CompilerParams(
            collective_id=0, has_side_effects=True, vmem_limit_bytes=60 * 1024 * 1024
        ),
    )(
        query_vectors,
        key_vectors,
        value_vectors,
        cos,
        sin,
        query_gain[None, :],
        key_gain[None, :],
        sinks,
        moe_rows,
        norm_gain[None, :],
        table,
        expert_gate,
        expert_up,
        expert_down,
        shared_gate,
        shared_up,
        shared_down,
    )


def choose(*args):
    ep, tp = lax.axis_size("ep"), lax.axis_size("tp")
    query, rows = args[0], args[6]
    kv_heads = args[1].shape[1] // HEAD_DIM
    tok, width = rows.shape
    cap = max(2, 3 * tok * TOP_K // (2 * ep))
    gathered = ep * tok * tp * width * 2
    chunks = query.shape[0] // WINDOW * kv_heads
    fits = (
        gathered <= 16 * 1024 * 1024
        and tp == 4
        and ep % 2 == 0
        and tok % 32 == 0
        and (2 * cap) % 16 == 0
        and cap % 8 == 0
        and query.shape[0] % GRID_W == 0
        and chunks % (ep // 2) == 0
    )
    return fast_shards(*args) if fits else shards(*args)


def solution(mesh):
    placed = (
        P("ep", "tp"),
        P("ep", "tp"),
        P("ep", "tp"),
        P(),
        P(),
        P("tp"),
        P("ep", "tp"),
        P(),
        P("ep", None),
        P("ep", None),
        P("ep", None, "tp"),
        P("ep", None, "tp"),
        P("ep", None, "tp"),
        P(None, "tp"),
        P(None, "tp"),
        P(None, "tp"),
    )
    return jax.shard_map(
        choose,
        mesh=mesh,
        in_specs=placed,
        out_specs=(P("ep", "tp"), P("ep", "tp")),
        check_vma=False,
    )
```

profile of v0, /device:TPU:0, one launch (start us, length us, event | category | flops | bytes accessed | tf_op | source)
XLA Modules:
  0.0 165.5 jit_solution(14399645126841926587)
XLA Ops:
  0.7 0.7 select_reduce_fusion
  1.4 0.6 pad.4.wt_hbm
  2.0 0.1 multiply_sine_fusion.1
  2.1 1.3 broadcast_in_dim.68.sink_ref
  3.5 0.2 multiply_sine_fusion
  3.8 1.1 pad_maximum_fusion.cos_ref
  4.9 0.1 bitcast_negate_fusion
  5.0 1.1 pad_maximum_fusion.1.sin_ref
  6.1 155.3 %shard_map.167 = (bf16[512,1024]{1,0:T(8,128)(2,1)}, bf16[160,1024]{1,0:T(8,128)(2,1)}) custom-call(bf16[512,1024]{1,0:T(8,128)(2,1)} %q_hbm.1, bf16[512,512]{1,0:T(8,128)(2,1)} %k_hbm.1, bf16[512,512]{1,0:T(8,128)(2,1)} %v_hbm.1, f32[768,128]{1,0:T(8,128)} %pad_maximum_fusion.cos_ref, f32[768,128]{1,0:T(8,128)} %pad_maximum_fusion.1.sin_ref, ...), custom_call_target="tpu_custom_call" | custom-call | tf_op jit(solution)/shard_map/pallas_call | solution.py:791
  161.5 2.3 %copy.20 = bf16[512,1024]{1,0:T(8,128)(2,1)} copy(bf16[512,1024]{1,0:T(8,128)(2,1)} %get-tuple-element.10) | data formatting | bytes 2097152
  163.8 1.7 %copy.21 = bf16[160,1024]{1,0:T(8,128)(2,1)} copy(bf16[160,1024]{1,0:T(8,128)(2,1)} %get-tuple-element.11) | data formatting | bytes 655360
  (7 shorter events, 0.1 us)
where the time goes:
time: 166 us; the launch traced here: 165 us
  Pallas kernels  155 us (93%)
  local copies, waits for them, and re-layouts  6.05 us (4%)
  other arithmetic  3.34 us (2%)
    pallas_call x1, Pallas kernels, fast_shards(): pl.pallas_call(functools.partial(moe_kernel, sizes), out_shape=(jax.Shape...  155 us
    unnamed x2, local copies, waits for them, and re-layouts  3.98 us

commit v1 on v0

--- a/solution.py
+++ b/solution.py
@@ -1,4 +1,5 @@
 import functools
+import math
 
 import jax
 import jax.numpy as jnp
@@ -194,27 +195,26 @@
 LANES = 128
 
 
-def moe_kernel(
+def line_kernel(
     sizes,
     q_hbm,
     k_hbm,
     v_hbm,
-    cos_ref,
-    sin_ref,
     qgain_ref,
     kgain_ref,
     sink_ref,
     x_hbm,
     gain_ref,
-    wt_hbm,
+    ids_ref,
+    rw_ref,
     gate_hbm,
     up_hbm,
     down_hbm,
     sgate_hbm,
     sup_hbm,
     sdown_hbm,
-    att_ref,
-    out_ref,
+    att_hbm,
+    out_hbm,
     xbuf,
     gate,
     up,
@@ -222,9 +222,16 @@
     sgate,
     sup,
     sdown,
+    qraw,
     qbuf,
+    kraw,
     kbuf,
     vbuf,
+    abuf,
+    obuf,
+    base,
+    cos_ref,
+    sin_ref,
     wbuf,
     scaled,
     factor,
@@ -235,17 +242,19 @@
     prx,
     qtx,
     qrx,
-    local_sem,
-    zs,
-    zr,
+    lsem,
+    asem,
+    osem,
+    zts,
+    ztr,
+    zds,
+    zdr,
     xs,
     xr,
     ys,
     yr,
-    dxs,
-    dxr,
-    dys,
-    dyr,
+    fs,
+    fr,
     ps,
     pr,
     hxs,
@@ -282,6 +291,26 @@
     hcut = (slots // 2 + 15) // 16 * 16
     row_c = pl.multiple_of(c * tok, 16)
     row_o = pl.multiple_of(other * tok, 16)
+    has_up, has_down = z < nz - 1, z > 0
+    is_end = (z == 0) | (z == nz - 1)
+    is_mid = jnp.logical_not(is_end)
+
+    def by_z(*values):
+        r = values[0]
+        for i in range(1, nz):
+            r = jnp.where(z == i, values[i], r)
+        return r
+
+    order = (z, by_z(1, 2, 1, 2), by_z(3, 3, 0, 0), by_z(2, 0, 3, 1))
+    k1, k2 = by_z(1, 2, 1, 2), by_z(2, 0, 3, 1)
+    k3, k4 = by_z(1, 0, 3, 2), by_z(3, 3, 0, 0)
+    k5, k6 = by_z(3, 2, 1, 0), by_z(2, 3, 0, 1)
+
+    def at_step(s):
+        r = order[0]
+        for i in range(1, nz):
+            r = jnp.where(s == i, order[i], r)
+        return r
 
     def rc(src, dst, s_sem, r_sem, dev):
         return pltpu.make_async_remote_copy(
@@ -293,13 +322,11 @@
             device_id_type=MESH,
         )
 
-    unit0 = xbuf.at[z, t, pl.ds(row_c, tok), :]
     loads = [
-        (x_hbm, unit0),
-        (wt_hbm, wbuf.at[e]),
-        (k_hbm, kbuf.at[pl.ds(WINDOW, tok_a), :]),
+        (x_hbm, xbuf.at[z, t, pl.ds(row_c, tok), :]),
+        (q_hbm, qraw),
+        (k_hbm, kraw.at[pl.ds(WINDOW, tok_a), :]),
         (v_hbm, vbuf.at[pl.ds(WINDOW, tok_a), :]),
-        (q_hbm, qbuf),
         (gate_hbm.at[0], gate),
         (up_hbm.at[0], up),
         (sgate_hbm, sgate),
@@ -307,61 +334,100 @@
         (down_hbm.at[0], down),
         (sdown_hbm, sdown),
     ]
-    copies = [
-        pltpu.make_async_copy(a, b, local_sem.at[i]) for i, (a, b) in enumerate(loads)
-    ]
-    for cp in copies:
-        cp.start()
+    copies = [pltpu.make_async_copy(a, b, lsem.at[i]) for i, (a, b) in enumerate(loads)]
 
     barrier = pltpu.get_barrier_semaphore()
     for d in range(1, ep):
         pl.semaphore_signal(barrier, inc=1, device_id=((e + d) % ep, t), device_id_type=MESH)
     for d in range(1, tp):
         pl.semaphore_signal(barrier, inc=1, device_id=(e, (t + d) % tp), device_id_type=MESH)
+    for cp in copies:
+        cp.start()
+
+    quarter = HEAD_DIM // 4
+    half_head = HEAD_DIM // 2
+    extent = tok_a + 2 * WINDOW
+    grid_rows = extent // GRID_W
+    first_row = (e * tok_a - WINDOW) // GRID_W
+
+    def angles(count, start):
+        lane = lax.broadcasted_iota(jnp.int32, (count, LANES), 1)
+        place = lax.broadcasted_iota(jnp.int32, (count, LANES), 0)
+        exponent = (lane % quarter).astype(F32) * (-4.0 / HEAD_DIM)
+        return (place + start).astype(F32) * jnp.exp(exponent * math.log(rotary_base))
+
+    row_pad = (grid_rows + 7) // 8 * 8
+    row_angles = angles(row_pad, first_row)
+    col_angles = angles(GRID_W, 0)
+    row_cos, row_sin = jnp.cos(row_angles), jnp.sin(row_angles)
+    col_cos, col_sin = jnp.cos(col_angles), jnp.sin(col_angles)
+    lane64 = lax.broadcasted_iota(jnp.int32, (GRID_W, LANES), 1)
+    sign = jnp.where(lane64 % half_head < quarter, -1.0, 1.0)
+    for g in range(grid_rows):
+        rows = slice(g * GRID_W, (g + 1) * GRID_W)
+        cos_ref[rows, :] = jnp.where(lane64 < half_head, row_cos[g : g + 1, :], col_cos)
+        sin_ref[rows, :] = jnp.where(lane64 < half_head, row_sin[g : g + 1, :], col_sin) * sign
+
+    padded_tok = wbuf.shape[2]
+    expert = lax.broadcasted_iota(jnp.int32, (tok, LANES), 1)
+    by_token = jnp.zeros((tok, LANES), F32)
+    for k in range(TOP_K):
+        by_token += jnp.where(ids_ref[:, k : k + 1] == expert, rw_ref[:, k : k + 1], 0.0)
+    if padded_tok > tok:
+        by_token = jnp.concatenate(
+            [by_token, jnp.zeros((padded_tok - tok, LANES), F32)], axis=0
+        )
+    wbuf[e] = by_token.T[:ep, :]
+
     pl.semaphore_wait(barrier, ep + tp - 2)
 
     def unit(zi, ti, row, first=0, count=tok):
         return xbuf.at[zi, ti, pl.ds(row + first, count), :]
 
-    def z_copy(d):
-        zi = (z + d) % nz
-        return rc(unit0, unit0, zs.at[d], zr.at[z], (zi * 2 + c, t))
-
-    def z_landed(zi):
+    up_z = jnp.minimum(z + 1, nz - 1) * 2 + c
+    down_z = jnp.maximum(z - 1, 0) * 2 + c
+
+    def zt_copy(zi, way):
         u = unit(zi, t, row_c)
-        return rc(u, u, zs.at[0], zr.at[zi], (e, xn))
-
-    def x_copy(zi):
-        u = unit(zi, t, row_c)
-        return rc(u, u, xs.at[zi], xr.at[zi], (e, xn))
-
-    def y_copy(zi):
-        u = unit(zi, t, row_c)
-        return rc(u, u, ys.at[zi], yr.at[zi], (e, yn))
-
-    def x_landed(zi):
-        u = unit(zi, xn, row_c)
-        return rc(u, u, xs.at[zi], xr.at[zi], (e, xn))
-
-    def y_landed(zi):
-        u = unit(zi, yn, row_c)
-        return rc(u, u, ys.at[zi], yr.at[zi], (e, yn))
-
-    def dy_copy(zi):
-        u = unit(zi, xn, row_c, 0, half)
-        return rc(u, u, dys.at[zi], dyr.at[zi], (e, yn))
-
-    def dx_copy(zi):
-        u = unit(zi, yn, row_c, half, half)
-        return rc(u, u, dxs.at[zi], dxr.at[zi], (e, xn))
-
-    def dy_landed(zi):
-        u = unit(zi, dn, row_c, 0, half)
-        return rc(u, u, dys.at[zi], dyr.at[zi], (e, yn))
-
-    def dx_landed(zi):
-        u = unit(zi, dn, row_c, half, half)
-        return rc(u, u, dxs.at[zi], dxr.at[zi], (e, xn))
+        return rc(u, u, zts.at[zi, way], ztr.at[zi], ((up_z, down_z)[way], t))
+
+    def zd_copy(zi, way):
+        u = unit(zi, dn, row_c)
+        return rc(u, u, zds.at[zi, way], zdr.at[zi], ((up_z, down_z)[way], t))
+
+    def along(zi, what):
+        @pl.when((zi <= z) & has_up)
+        def _():
+            what(0)
+
+        @pl.when((zi >= z) & has_down)
+        def _():
+            what(1)
+
+    def send_t(zi):
+        along(zi, lambda way: zt_copy(zi, way).start())
+
+    def send_d(zi):
+        along(zi, lambda way: zd_copy(zi, way).start())
+
+    def xy_copy(zi, which, piece, first, count):
+        u = unit(zi, t, row_c, first, count)
+        sems = (xs, xr) if which == 0 else (ys, yr)
+        return rc(u, u, sems[0].at[zi, piece], sems[1].at[zi, piece], (e, (xn, yn)[which]))
+
+    def xy_landed(zi, which, piece, first, count):
+        u = unit(zi, (xn, yn)[which], row_c, first, count)
+        sems = (xs, xr) if which == 0 else (ys, yr)
+        return rc(u, u, sems[0].at[zi, piece], sems[1].at[zi, piece], (e, (xn, yn)[which]))
+
+    def diagonal(which):
+        source, first = ((yn, half), (xn, 0))[which]
+        u = unit(z, source, row_c, first, half)
+        return rc(u, u, fs.at[which], fr.at[which], (e, (xn, yn)[which]))
+
+    def diagonal_landed(which):
+        u = unit(z, dn, row_c, (half, 0)[which], half)
+        return rc(u, u, fs.at[which], fr.at[which], (e, (xn, yn)[which]))
 
     def p_copy(zi, ti):
         u = unit(zi, ti, row_c)
@@ -371,37 +437,27 @@
         u = unit(zi, ti, row_o)
         return rc(u, u, ps.at[zi, ti], pr.at[zi, ti], (partner, t))
 
-    def hx_copy(zi):
-        u = hbuf.at[zi, t]
-        return rc(u, u, hxs.at[zi], hxr.at[zi], (e, xn))
-
-    def hy_copy(zi):
-        u = hbuf.at[zi, t]
-        return rc(u, u, hys.at[zi], hyr.at[zi], (e, yn))
-
-    def hx_landed(zi):
-        u = hbuf.at[zi, xn]
-        return rc(u, u, hxs.at[zi], hxr.at[zi], (e, xn))
-
-    def hy_landed(zi):
-        u = hbuf.at[zi, yn]
-        return rc(u, u, hys.at[zi], hyr.at[zi], (e, yn))
-
-    def gy_copy(zi):
-        u = hbuf.at[zi, xn, pl.ds(0, hcut), :]
-        return rc(u, u, gys.at[zi], gyr.at[zi], (e, yn))
-
-    def gx_copy(zi):
-        u = hbuf.at[zi, yn, pl.ds(hcut, slots - hcut), :]
-        return rc(u, u, gxs.at[zi], gxr.at[zi], (e, xn))
-
-    def gy_landed(zi):
-        u = hbuf.at[zi, dn, pl.ds(0, hcut), :]
-        return rc(u, u, gys.at[zi], gyr.at[zi], (e, yn))
-
-    def gx_landed(zi):
-        u = hbuf.at[zi, dn, pl.ds(hcut, slots - hcut), :]
-        return rc(u, u, gxs.at[zi], gxr.at[zi], (e, xn))
+    h_parts = ((0, hcut), (hcut, slots - hcut))
+
+    def h_copy(zi, which, piece):
+        u = hbuf.at[zi, t, pl.ds(*h_parts[piece]), :]
+        sems = (hxs, hxr) if which == 0 else (hys, hyr)
+        return rc(u, u, sems[0].at[zi, piece], sems[1].at[zi, piece], (e, (xn, yn)[which]))
+
+    def h_landed(zi, which, piece):
+        u = hbuf.at[zi, (xn, yn)[which], pl.ds(*h_parts[piece]), :]
+        sems = (hxs, hxr) if which == 0 else (hys, hyr)
+        return rc(u, u, sems[0].at[zi, piece], sems[1].at[zi, piece], (e, (xn, yn)[which]))
+
+    def g_copy(zi, which):
+        u = hbuf.at[zi, (yn, xn)[which], pl.ds(*h_parts[1 - which]), :]
+        sems = (gxs, gxr) if which == 0 else (gys, gyr)
+        return rc(u, u, sems[0].at[zi], sems[1].at[zi], (e, (xn, yn)[which]))
+
+    def g_landed(zi, which):
+        u = hbuf.at[zi, dn, pl.ds(*h_parts[1 - which]), :]
+        sems = (gxs, gxr) if which == 0 else (gys, gyr)
+        return rc(u, u, sems[0].at[zi], sems[1].at[zi], (e, (xn, yn)[which]))
 
     def s_copy(d):
         u = shbuf.at[t]
@@ -419,120 +475,161 @@
         u = wbuf.at[ei]
         return rc(u, u, ws.at[0], wr.at[ei], (partner, t))
 
-    after, before = (e + 1) % ep, (e + ep - 1) % ep
-    tail = pl.ds(tok_a, WINDOW)
-    first = pl.ds(WINDOW, WINDOW)
-    low = pl.ds(0, WINDOW)
-    high = pl.ds(WINDOW + tok_a, WINDOW)
-    halos = [
-        rc(kbuf.at[tail, :], kbuf.at[low, :], ks.at[0], kr.at[0], (after, t)),
-        rc(kbuf.at[first, :], kbuf.at[high, :], ks.at[1], kr.at[1], (before, t)),
-        rc(vbuf.at[tail, :], vbuf.at[low, :], ks.at[2], kr.at[2], (after, t)),
-        rc(vbuf.at[first, :], vbuf.at[high, :], ks.at[3], kr.at[3], (before, t)),
+    after, before = jnp.minimum(e + 1, ep - 1), jnp.maximum(e - 1, 0)
+    tail, first = pl.ds(tok_a, WINDOW), pl.ds(WINDOW, WINDOW)
+    low, high = pl.ds(0, WINDOW), pl.ds(WINDOW + tok_a, WINDOW)
+    halo_up = [
+        rc(b.at[tail, :], b.at[low, :], ks.at[i], kr.at[i], (after, t))
+        for i, b in enumerate((kraw, vbuf))
     ]
-
-    def pp_copy(zi):
-        return rc(pbuf.at[zi, other], prx.at[zi], pps.at[zi], ppr.at[zi], (partner, t))
-
-    def qq_copy(zi):
-        return rc(qtx.at[zi], qrx.at[z], qqs.at[zi], qqr.at[z], (zi * 2 + c, t))
-
-    def qq_landed(zi):
-        return rc(qrx.at[zi], qrx.at[zi], qqs.at[zi], qqr.at[zi], (partner, t))
+    halo_down = [
+        rc(b.at[first, :], b.at[high, :], ks.at[2 + i], kr.at[2 + i], (before, t))
+        for i, b in enumerate((kraw, vbuf))
+    ]
+
+    def pp_copy(zi, n):
+        return rc(pbuf.at[zi, n, other], prx.at[zi, n], pps.at[zi, n], ppr.at[zi, n], (partner, t))
+
+    def qq_copy(zi, n):
+        return rc(qtx.at[zi, n], qrx.at[z, n], qqs.at[zi, n], qqr.at[z, n], (zi * 2 + c, t))
+
+    def qq_landed(zi, n):
+        return rc(qrx.at[zi, n], qrx.at[zi, n], qqs.at[zi, n], qqr.at[zi, n], (partner, t))
 
     copies[0].wait()
-    x_copy(z).start()
-    y_copy(z).start()
-    for d in range(1, nz):
-        z_copy(d).start()
+    xy_copy(z, 0, 0, 0, half).start()
+    xy_copy(z, 1, 1, half, half).start()
+    send_t(z)
+    xy_copy(z, 0, 1, half, half).start()
+    xy_copy(z, 1, 0, 0, half).start()
     p_copy(z, t).start()
-    copies[1].wait()
     for d in range(1, ep):
         w_copy(d).start()
-    copies[2].wait()
-    copies[3].wait()
-    for h in halos:
-        h.start()
-    copies[4].wait()
-
-    lane = lax.broadcasted_iota(jnp.int32, (WINDOW, LANES), 1)
-    leading = (lane % (HEAD_DIM // 2)) < HEAD_DIM // 4
-
-    def turn(block, head_gain, table_rows):
+    for i in (1, 2, 3):
+        copies[i].wait()
+
+    @pl.when(c == 0)
+    def _():
+        for h in halo_up:
+            h.start()
+
+    @pl.when(c == 1)
+    def _():
+        for h in halo_down:
+            h.start()
+
+    @pl.when(e == 0)
+    def _():
+        kraw[0:WINDOW, :] = jnp.zeros((WINDOW, kv_heads * HEAD_DIM), BF16)
+        vbuf[0:WINDOW, :] = jnp.zeros((WINDOW, kv_heads * HEAD_DIM), BF16)
+
+    @pl.when(e == ep - 1)
+    def _():
+        end = slice(WINDOW + tok_a, 2 * WINDOW + tok_a)
+        kraw[end, :] = jnp.zeros((WINDOW, kv_heads * HEAD_DIM), BF16)
+        vbuf[end, :] = jnp.zeros((WINDOW, kv_heads * HEAD_DIM), BF16)
+
+    trows = 64
+    lane = lax.broadcasted_iota(jnp.int32, (trows, LANES), 1)
+    leading = (lane % half_head) < quarter
+
+    def turn(block, head_gain, cos, sin):
         v = block.astype(F32)
         v = v * lax.rsqrt(jnp.mean(v * v, axis=-1, keepdims=True) + epsilon) * head_gain
         swapped = jnp.where(
             leading,
-            pltpu.roll(v, HEAD_DIM - HEAD_DIM // 4, 1),
-            pltpu.roll(v, HEAD_DIM // 4, 1),
+            pltpu.roll(v, HEAD_DIM - quarter, 1),
+            pltpu.roll(v, quarter, 1),
         )
-        return (v * cos_ref[table_rows, :] + swapped * sin_ref[table_rows, :]).astype(BF16)
+        return (v * cos + swapped * sin).astype(BF16)
 
     heads = kv_heads * group
 
-    def turn_q(i, carry):
-        rows = pl.ds(pl.multiple_of(i * WINDOW, WINDOW), WINDOW)
-        table = pl.ds(pl.multiple_of((i + 1) * WINDOW, WINDOW), WINDOW)
-        for h in range(heads):
-            cols = slice(h * HEAD_DIM, (h + 1) * HEAD_DIM)
-            qbuf[rows, cols] = turn(qbuf[rows, cols], qgain_ref[...], table)
-        return carry
+    def turn_rows(src, dst, count, head_gain, lo, hi, shift):
+        def body(i, carry):
+            rows = pl.ds(pl.multiple_of(i * trows, trows), trows)
+            table = pl.ds(pl.multiple_of(i * trows + shift, trows), trows)
+            cos, sin = cos_ref[table, :], sin_ref[table, :]
+            for h in range(count):
+                cols = slice(h * HEAD_DIM, (h + 1) * HEAD_DIM)
+                dst[rows, cols] = turn(src[rows, cols], head_gain, cos, sin)
+            return carry
+
+        lax.fori_loop(lo, hi, body, 0)
 
     nq = tok_a // WINDOW
-    lax.fori_loop(0, nq, turn_q, 0)
-
-    def forward_z(zi):
-        z_landed(zi).wait_recv()
-        x_copy(zi).start()
-        y_copy(zi).start()
+    per_window = WINDOW // trows
+    turn_rows(qraw, qbuf, heads, qgain_ref[...], 0, nq * per_window, WINDOW)
+
+    xy_landed(z, 0, 0, 0, half).wait_recv()
+    diagonal(1).start()
+    xy_landed(z, 1, 1, half, half).wait_recv()
+    diagonal(0).start()
+
+    turn_rows(kraw, kbuf, kv_heads, kgain_ref[...], per_window, (nq + 1) * per_window, 0)
+
+    def take_t(zi):
+        u = unit(zi, t, row_c)
+        rc(u, u, zts.at[zi, 0], ztr.at[zi], (e, xn)).wait_recv()
+        xy_copy(zi, 0, 0, 0, tok).start()
+        xy_copy(zi, 1, 0, 0, tok).start()
+        send_t(zi)
         p_copy(zi, t).start()
 
-    forward_z((z + 1) % nz)
-
-    for h in halos:
-        h.wait()
-
-    def turn_k(i, carry):
-        rows = pl.ds(pl.multiple_of(i * WINDOW, WINDOW), WINDOW)
-        for h in range(kv_heads):
-            cols = slice(h * HEAD_DIM, (h + 1) * HEAD_DIM)
-            kbuf[rows, cols] = turn(kbuf[rows, cols], kgain_ref[...], rows)
-        return carry
-
-    lax.fori_loop(0, nq + 2, turn_k, 0)
-    for d in range(1, ep):
-        w_landed((e + d) % ep).wait_recv()
-    for cp in copies[5:]:
-        cp.wait()
+    def wait_d(zi):
+        u = unit(zi, dn, row_c)
+        rc(u, u, zds.at[zi, 0], zdr.at[zi], (e, xn)).wait_recv()
+        p_copy(zi, dn).start()
+
+    def take_xy(zi):
+        xy_landed(zi, 0, 0, 0, tok).wait_recv()
+        p_copy(zi, xn).start()
+        xy_landed(zi, 1, 0, 0, tok).wait_recv()
+        p_copy(zi, yn).start()
+
+    take_t(k1)
+
+    @pl.when(is_mid)
+    def _():
+        take_t(k2)
 
     span = 3 * WINDOW
-
-    def attend(i, carry):
-        qb, kh = i // kv_heads, i % kv_heads
+    near = lax.broadcasted_iota(jnp.int32, (WINDOW, WINDOW), 1)
+    mine = lax.broadcasted_iota(jnp.int32, (WINDOW, WINDOW), 0)
+    exp_scale = HEAD_DIM ** (-0.5)
+
+    def attend(qb):
         rows = pl.ds(pl.multiple_of(qb * WINDOW, WINDOW), WINDOW)
         keys = pl.ds(pl.multiple_of(qb * WINDOW, WINDOW), span)
-        kcols = pl.ds(pl.multiple_of(kh * HEAD_DIM, HEAD_DIM), HEAD_DIM)
-        near = lax.broadcasted_iota(jnp.int32, (WINDOW, span), 1)
-        mine = lax.broadcasted_iota(jnp.int32, (WINDOW, span), 0)
-        pos = e * tok_a + (qb - 1) * WINDOW + near
-        inside = (
-            (near - mine >= 0) & (near - mine <= 2 * WINDOW) & (pos >= 0) & (pos < ep * tok_a)
-        )
-        kk = kbuf[keys, kcols]
-        vv = vbuf[keys, kcols]
-        for g in range(group):
-            qcols = pl.ds(
-                pl.multiple_of((kh * group + g) * HEAD_DIM, HEAD_DIM), HEAD_DIM
-            )
-            scores = lax.dot_general(
-                qbuf[rows, qcols], kk, (((1,), (1,)), ((), ())), preferred_element_type=F32
-            )
-            raised = jnp.where(inside, jnp.exp(scores * HEAD_DIM ** (-0.5)), 0.0)
-            sink = jnp.exp(sink_ref[kh * group + g])
-            total = jnp.sum(raised, axis=-1, keepdims=True) + sink[0:1, 0:1]
-            weights = (raised * (1.0 / total)).astype(BF16)
-            att_ref[rows, qcols] = jnp.dot(weights, vv, preferred_element_type=F32).astype(BF16)
-        return carry
+        in_low = (near >= mine) & ((e > 0) | (qb > 0))
+        in_high = (near <= mine) & ((e < ep - 1) | (qb < nq - 1))
+        sinks = jnp.exp(sink_ref[...])
+        for kh in range(kv_heads):
+            kcols = slice(kh * HEAD_DIM, (kh + 1) * HEAD_DIM)
+            kk = kbuf[keys, kcols]
+            vv = vbuf[keys, kcols]
+            for g in range(group):
+                h = kh * group + g
+                qcols = slice(h * HEAD_DIM, (h + 1) * HEAD_DIM)
+                scores = lax.dot_general(
+                    qbuf[rows, qcols], kk, (((1,), (1,)), ((), ())), preferred_element_type=F32
+                )
+                raised = jnp.exp(scores * exp_scale)
+                parts = [
+                    jnp.where(in_low, raised[:, :WINDOW], 0.0),
+                    raised[:, WINDOW : 2 * WINDOW],
+                    jnp.where(in_high, raised[:, 2 * WINDOW :], 0.0),
+                ]
+                total = jnp.sum(parts[0] + parts[1] + parts[2], axis=-1, keepdims=True)
+                inverse = 1.0 / (total + sinks[:, h : h + 1])
+                weights = jnp.concatenate([(p * inverse).astype(BF16) for p in parts], axis=1)
+                abuf[rows, qcols] = jnp.dot(
+                    weights, vv, preferred_element_type=F32
+                ).astype(BF16)
+
+    def att_copy(qb):
+        rows = pl.ds(pl.multiple_of(qb * WINDOW, WINDOW), WINDOW)
+        return pltpu.make_async_copy(abuf.at[rows, :], att_hbm.at[rows, :], asem.at[qb])
 
     upper = (
         lax.broadcasted_iota(jnp.int32, (tok, tok), 0)
@@ -601,6 +698,8 @@
         shbuf[t] = silu_pair(g, u, factor[rows, 0:1]).astype(BF16)
 
     ctile = min(256, columns)
+    chalf = columns // 2
+    per_half = chalf // ctile
 
     def down_pair(zi):
         picked = [picks(zi * 2 + ci) for ci in range(2)]
@@ -616,6 +715,8 @@
                     preferred_element_type=F32,
                 )
             weighted = acc.astype(BF16).astype(F32) * slot_weight
+            part = n // per_half
+            put = pl.ds(pl.multiple_of((n % per_half) * ctile, ctile), ctile)
             for ci in range(2):
                 spread = lax.dot_general(
                     picked[ci][0].astype(BF16),
@@ -623,37 +724,120 @@
                     (((0,), (0,)), ((), ())),
                     preferred_element_type=F32,
                 )
-                pbuf[zi, ci, :, cols] = spread.astype(BF16)
+                pbuf[zi, part, ci, :, put] = spread.astype(BF16)
+
+            @pl.when(n % per_half == per_half - 1)
+            def _():
+                pp_copy(zi, part).start()
+
             return carry
 
         lax.fori_loop(0, columns // ctile, columns_of, 0)
 
-    per_step = nq * kv_heads // nz
+    qorder = (1, 2, 0, 3)
 
     def step(s, carry):
+        zi = at_step(s)
+
+        @pl.when(s == 1)
+        def _():
+            @pl.when(is_end)
+            def _():
+                take_t(k2)
+
+        @pl.when(s == 2)
+        def _():
+            @pl.when(is_mid)
+            def _():
+                wait_d(k6)
+                send_d(k6)
+                send_d(k5)
+
+            @pl.when(e > 0)
+            def _():
+                for h in halo_up:
+                    h.wait_recv()
+
+            @pl.when(e < ep - 1)
+            def _():
+                for h in halo_down:
+                    h.wait_recv()
+
+            turn_rows(kraw, kbuf, kv_heads, kgain_ref[...], 0, per_window, 0)
+            last = (nq + 1) * per_window
+            turn_rows(kraw, kbuf, kv_heads, kgain_ref[...], last, last + per_window, 0)
+
+        @pl.when((s == 1) | (s == 3))
+        def _():
+            take_xy(zi)
+
         @pl.when(s < nz)
         def _():
-            lax.fori_loop(s * per_step, (s + 1) * per_step, attend, 0)
-            zi = (z + s) % nz
-            x_landed(zi).wait_recv()
-            dy_copy(zi).start()
-            p_copy(zi, xn).start()
-            y_landed(zi).wait_recv()
-            dx_copy(zi).start()
-            p_copy(zi, yn).start()
-
-            @pl.when(s + 2 < nz)
+            qb = qorder[0]
+            for i in range(1, nz):
+                qb = jnp.where(s == i, qorder[i], qb)
+            attend(qb)
+            att_copy(qb).start()
+
+            @pl.when(s == 0)
             def _():
-                forward_z((z + s + 2) % nz)
-
-            dy_landed(zi).wait_recv()
-            dx_landed(zi).wait_recv()
-            p_copy(zi, dn).start()
+                for piece, which in ((1, 0), (0, 1)):
+                    xy_landed(z, which, piece, piece * half, half).wait_recv()
+                    p_copy(z, (xn, yn)[which]).start()
+                for which in range(2):
+                    diagonal_landed(which).wait_recv()
+                p_copy(z, dn).start()
+                send_d(z)
+
+                @pl.when((c == 1) & (e < ep - 1))
+                def _():
+                    for h in halo_up:
+                        h.start()
+
+                @pl.when((c == 0) & (e > 0))
+                def _():
+                    for h in halo_down:
+                        h.start()
+
+                for d in range(1, ep):
+                    w_landed((e + d) % ep).wait_recv()
+                for cp in copies[4:]:
+                    cp.wait()
+
+            @pl.when(s == 1)
+            def _():
+                wait_d(k3)
+                send_d(k3)
+
+                @pl.when(is_mid)
+                def _():
+                    take_t(k4)
+                    wait_d(k5)
+
+            @pl.when(s == 2)
+            def _():
+                take_xy(zi)
+
+                @pl.when(is_end)
+                def _():
+                    wait_d(k5)
+
+            @pl.when((s == 3) & is_end)
+            def _():
+                wait_d(k6)
+
             for ti in range(tp):
                 p_landed(zi, ti).wait_recv()
             project_pair(zi)
-            hx_copy(zi).start()
-            hy_copy(zi).start()
+
+            @pl.when((s == 1) & is_end)
+            def _():
+                take_t(k4)
+
+            h_copy(zi, 0, 0).start()
+            h_copy(zi, 1, 1).start()
+            h_copy(zi, 0, 1).start()
+            h_copy(zi, 1, 0).start()
 
             @pl.when(s == 0)
             def _():
@@ -663,63 +847,103 @@
 
         @pl.when((s >= 1) & (s < nz + 1))
         def _():
-            zi = (z + s - 1) % nz
-            hx_landed(zi).wait_recv()
-            gy_copy(zi).start()
-            hy_landed(zi).wait_recv()
-            gx_copy(zi).start()
-
-        @pl.when((s >= 2) & (s < nz + 2))
+            zp = at_step(s - 1)
+            h_landed(zp, 0, 0).wait_recv()
+            g_copy(zp, 1).start()
+            h_landed(zp, 1, 1).wait_recv()
+            g_copy(zp, 0).start()
+
+        @pl.when((s >= 3) & (s < nz + 3))
         def _():
-            zi = (z + s - 2) % nz
-            gy_landed(zi).wait_recv()
-            gx_landed(zi).wait_recv()
-            down_pair(zi)
-            pp_copy(zi).start()
-            pp_copy(zi).wait_recv()
-            qtx[zi] = (pbuf[zi, c].astype(F32) + prx[zi].astype(F32)).astype(BF16)
-
-            @pl.when(s > 2)
-            def _():
-                qq_copy(zi).start()
+            zq = at_step(s - 3)
+            h_landed(zq, 0, 1).wait_recv()
+            h_landed(zq, 1, 0).wait_recv()
+            g_landed(zq, 0).wait_recv()
+            g_landed(zq, 1).wait_recv()
+            down_pair(zq)
+            for n in range(2):
+                pp_copy(zq, n).wait_recv()
+                qtx[zq, n] = (pbuf[zq, n, c].astype(F32) + prx[zq, n].astype(F32)).astype(BF16)
+
+                @pl.when(s > 3)
+                def _():
+                    qq_copy(zq, n).start()
 
         return carry
 
-    lax.fori_loop(0, nz + 2, step, 0)
+    lax.fori_loop(0, nz + 3, step, 0)
 
     for d in range(1, tp):
         s_landed((t + d) % tp).wait_recv()
-    for d in range(1, nz):
-        qq_landed((z + d) % nz).wait_recv()
     for n in range(columns // ctile):
         cols = slice(n * ctile, (n + 1) * ctile)
-        acc = qtx[z, :, cols].astype(F32)
-        for d in range(1, nz):
-            acc += qrx[(z + d) % nz, :, cols].astype(F32)
+        put = slice(n % per_half * ctile, (n % per_half + 1) * ctile)
+        acc = qtx[z, n // per_half, :, put].astype(F32)
         for ti in range(tp):
             acc += jnp.dot(
                 shbuf[ti],
                 sdown[ti * sunits : (ti + 1) * sunits, cols],
                 preferred_element_type=F32,
             )
-        out_ref[:, cols] = acc.astype(BF16)
-
-    for d in range(1, nz):
-        z_copy(d).wait_send()
-        qq_copy((z + d) % nz).wait_send()
+        base[:, cols] = acc
+
+    outs = []
+    for n in range(2):
+        for i in range(1, nz):
+            qq_landed(order[i], n).wait_recv()
+        cols = slice(n * chalf, (n + 1) * chalf)
+        acc = base[:, cols]
+        for i in range(1, nz):
+            acc += qrx[order[i], n].astype(F32)
+        obuf[n] = acc.astype(BF16)
+        outs.append(pltpu.make_async_copy(obuf.at[n], out_hbm.at[:, cols], osem.at[n]))
+        outs[-1].start()
+
+    def drain(zi, carry):
+        along(zi, lambda way: zt_copy(zi, way).wait_send())
+        along(zi, lambda way: zd_copy(zi, way).wait_send())
+        for which in range(2):
+            g_copy(zi, which).wait_send()
+            for piece in range(2):
+                h_copy(zi, which, piece).wait_send()
+        for n in range(2):
+            pp_copy(zi, n).wait_send()
+        for ti in range(tp):
+            p_copy(zi, ti).wait_send()
+
+        @pl.when(zi != z)
+        def _():
+            for which in range(2):
+                xy_copy(zi, which, 0, 0, tok).wait_send()
+            for n in range(2):
+                qq_copy(zi, n).wait_send()
+
+        return carry
+
+    lax.fori_loop(0, nz, drain, 0)
+    for which in range(2):
+        diagonal(which).wait_send()
+        for piece in range(2):
+            xy_copy(z, which, piece, piece * half, half).wait_send()
     for d in range(1, tp):
         s_copy(d).wait_send()
     for d in range(1, ep):
         w_copy(d).wait_send()
 
-    def drain(zi, carry):
-        for kind in (x_copy, y_copy, dx_copy, dy_copy, hx_copy, hy_copy, gx_copy, gy_copy, pp_copy):
-            kind(zi).wait_send()
-        for ti in range(tp):
-            p_copy(zi, ti).wait_send()
-        return carry
-
-    lax.fori_loop(0, nz, drain, 0)
+    @pl.when(e < ep - 1)
+    def _():
+        for h in halo_up:
+            h.wait_send()
+
+    @pl.when(e > 0)
+    def _():
+        for h in halo_down:
+            h.wait_send()
+
+    for qb in range(nq):
+        att_copy(qb).wait()
+    for cp in outs:
+        cp.wait()
 
 
 def fast_shards(
@@ -753,49 +977,25 @@
     sunits = shared_gate.shape[1]
     sizes = (ep, tp, nz, tok, width, cap, tok_a, kv_heads, group, units, columns, sunits)
     full = tp * width
-
     extent = tok_a + 2 * WINDOW
-    first_row = (lax.axis_index("ep") * tok_a - WINDOW) // GRID_W
-    grid_rows = extent // GRID_W
-    quarter = HEAD_DIM // 4
-    inverse = rotary_base ** (-4.0 * jnp.arange(quarter, dtype=jnp.int32).astype(F32) / HEAD_DIM)
-    row_ids = first_row + jnp.arange(grid_rows, dtype=jnp.int32)
-    grid_row = row_ids.astype(F32)[:, None] * inverse
-    grid_col = jnp.arange(GRID_W, dtype=jnp.int32).astype(F32)[:, None] * inverse
-
-    def by_row(a):
-        return jnp.broadcast_to(a[:, None, :], (grid_rows, GRID_W, quarter)).reshape(extent, quarter)
-
-    def by_col(a):
-        return jnp.broadcast_to(a[None], (grid_rows, GRID_W, quarter)).reshape(extent, quarter)
-
-    cr, sr = by_row(jnp.cos(grid_row)), by_row(jnp.sin(grid_row))
-    cc, sc = by_col(jnp.cos(grid_col)), by_col(jnp.sin(grid_col))
-    cos = jnp.concatenate([cr, cr, cc, cc], axis=-1)
-    sin = jnp.concatenate([-sr, sr, -sc, sc], axis=-1)
-
-    experts = jnp.arange(ep, dtype=jnp.int32)
-    table = jnp.sum(
-        jnp.where(expert_ids.T[None, :, :] == experts[:, None, None], route_weights.T[None], 0.0),
-        axis=1,
-    )
     padded_tok = (tok + LANES - 1) // LANES * LANES
-    table = jnp.pad(table, ((0, 0), (0, padded_tok - tok)))
-    sinks = jnp.broadcast_to(sink_logits[:, None, None], (heads, 8, LANES))
+    nq = tok_a // WINDOW
 
     vm = pl.BlockSpec(memory_space=pltpu.VMEM)
     hb = pl.BlockSpec(memory_space=pl.ANY)
     dma = pltpu.SemaphoreType.DMA
     slots = 2 * cap
-    zz = [dma((nz,))] * 2
+    kvw = kv_heads * HEAD_DIM
+    qw = heads * HEAD_DIM
+    one, two, four = [dma((nz,))] * 2, [dma((nz, 2))] * 2, [dma((nz, tp))] * 2
     return pl.pallas_call(
-        functools.partial(moe_kernel, sizes),
+        functools.partial(line_kernel, sizes),
         out_shape=(
-            jax.ShapeDtypeStruct((tok_a, heads * HEAD_DIM), BF16),
+            jax.ShapeDtypeStruct((tok_a, qw), BF16),
             jax.ShapeDtypeStruct((tok, columns), BF16),
         ),
-        in_specs=[hb, hb, hb, vm, vm, vm, vm, vm, hb, vm, hb, hb, hb, hb, hb, hb, hb],
-        out_specs=(vm, vm),
+        in_specs=[hb, hb, hb, vm, vm, vm, hb, vm, vm, vm, hb, hb, hb, hb, hb, hb],
+        out_specs=(hb, hb),
         scratch_shapes=[
             pltpu.VMEM((nz, tp, 2 * tok, width), BF16),
             pltpu.VMEM((full, units), BF16),
@@ -804,28 +1004,43 @@
             pltpu.VMEM((full, sunits), BF16),
             pltpu.VMEM((full, sunits), BF16),
             pltpu.VMEM((tp * sunits, columns), BF16),
-            pltpu.VMEM((tok_a, heads * HEAD_DIM), BF16),
-            pltpu.VMEM((extent, kv_heads * HEAD_DIM), BF16),
-            pltpu.VMEM((extent, kv_heads * HEAD_DIM), BF16),
+            pltpu.VMEM((tok_a, qw), BF16),
+            pltpu.VMEM((tok_a, qw), BF16),
+            pltpu.VMEM((extent, kvw), BF16),
+            pltpu.VMEM((extent, kvw), BF16),
+            pltpu.VMEM((extent, kvw), BF16),
+            pltpu.VMEM((tok_a, qw), BF16),
+            pltpu.VMEM((2, tok, columns // 2), BF16),
+            pltpu.VMEM((tok, columns), F32),
+            pltpu.VMEM((extent, LANES), F32),
+            pltpu.VMEM((extent, LANES), F32),
             pltpu.VMEM((ep, ep, padded_tok), F32),
             pltpu.VMEM((2 * tok, full), BF16),
             pltpu.VMEM((2 * tok, LANES), F32),
             pltpu.VMEM((2 * tok, units), BF16),
             pltpu.VMEM((nz, tp, slots, units), BF16),
             pltpu.VMEM((tp, tok, sunits), BF16),
-            pltpu.VMEM((nz, 2, tok, columns), BF16),
-            pltpu.VMEM((nz, tok, columns), BF16),
-            pltpu.VMEM((nz, tok, columns), BF16),
-            pltpu.VMEM((nz, tok, columns), BF16),
-            dma((11,)),
+            pltpu.VMEM((nz, 2, 2, tok, columns // 2), BF16),
+            pltpu.VMEM((nz, 2, tok, columns // 2), BF16),
+            pltpu.VMEM((nz, 2, tok, columns // 2), BF16),
+            pltpu.VMEM((nz, 2, tok, columns // 2), BF16),
+            dma((10,)),
+            dma((nq,)),
+            dma((2,)),
+            dma((nz, 2)),
+            dma((nz,)),
+            dma((nz, 2)),
+            dma((nz,)),
         ]
-        + zz * 5
-        + [dma((nz, tp))] * 2
-        + zz * 4
+        + two * 2
+        + [dma((2,))] * 2
+        + four
+        + two * 2
+        + one * 2
         + [dma((tp,))] * 2
         + [dma((ep,))] * 2
         + [dma((4,))] * 2
-        + zz * 2,
+        + two * 2,
         compiler_params=pltpu.CompilerParams(
             collective_id=0, has_side_effects=True, vmem_limit_bytes=60 * 1024 * 1024
         ),
@@ -833,14 +1048,13 @@
         query_vectors,
         key_vectors,
         value_vectors,
-        cos,
-        sin,
         query_gain[None, :],
         key_gain[None, :],
-        sinks,
+        sink_logits[None, :],
         moe_rows,
         norm_gain[None, :],
-        table,
+        expert_ids,
+        route_weights,
         expert_gate,
         expert_up,
         expert_down,
@@ -857,16 +1071,16 @@
     tok, width = rows.shape
     cap = max(2, 3 * tok * TOP_K // (2 * ep))
     gathered = ep * tok * tp * width * 2
-    chunks = query.shape[0] // WINDOW * kv_heads
     fits = (
         gathered <= 16 * 1024 * 1024
         and tp == 4
-        and ep % 2 == 0
-        and tok % 32 == 0
+        and ep == 8
         and (2 * cap) % 16 == 0
         and cap % 8 == 0
         and query.shape[0] % GRID_W == 0
-        and chunks % (ep // 2) == 0
+        and query.shape[0] == WINDOW * (ep // 2)
+        and tok % 32 == 0
+        and tok <= 2 * LANES
     )
     return fast_shards(*args) if fits else shards(*args)
 

time: 166 us -> 111 us (0.67)
  Pallas kernels: 155 us -> 104 us
  other arithmetic: 3.34 us -> 0 us
    pallas_call x1, Pallas kernels: 155 us -> 104 us  [fast_shards(): pl.pallas_call(functools.partial(line_kernel, sizes), out_shape=(jax.Shap...]
    unnamed x2 -> x4, local copies, waits for them, and re-layouts: 3.98 us -> 6.85 us
    concatenate x2 -> x0, other arithmetic: 2.25 us -> none  [the longest x1 1.13 us: fast_shards(): sin = jnp.concatenate([-sr, sr, -sc, sc], axis=-1)]
where the time goes in v1:
time: 111 us
  Pallas kernels  104 us (94%)
  local copies, waits for them, and re-layouts  6.85 us (6%)
    pallas_call x1, Pallas kernels, fast_shards(): pl.pallas_call(functools.partial(line_kernel, sizes), out_shape=(jax.Shap...  104 us
    unnamed x4, local copies, waits for them, and re-layouts  6.85 us

profile of v1, /device:TPU:0, one launch (start us, length us, event | category | flops | bytes accessed | tf_op | source)
XLA Modules:
  0.0 111.2 jit_solution(3827681295516780260)
XLA Ops:
  0.6 1.4 %copy.18.ids_ref = s32[160,4]{1,0:T(8,128)} copy(s32[160,4]{0,1:T(4,128)} %param.24) | data formatting | bytes 5120 | tf_op args[8]
  2.1 1.4 %copy.19.rw_ref = f32[160,4]{1,0:T(8,128)} copy(f32[160,4]{0,1:T(4,128)} %param.25) | data formatting | bytes 5120 | tf_op args[9]
  3.5 103.7 %shard_map.167 = (bf16[512,1024]{1,0:T(8,128)(2,1)}, bf16[160,1024]{1,0:T(8,128)(2,1)}) custom-call(bf16[512,1024]{1,0:T(8,128)(2,1)} %q_hbm.1, bf16[512,512]{1,0:T(8,128)(2,1)} %k_hbm.1, bf16[512,512]{1,0:T(8,128)(2,1)} %v_hbm.1, f32[1,128]{1,0:T(1,128)} %bitcast.5, f32[1,128]{1,0:T(1,128)} %bitcast.6, f32[1,8]{1,0:T(1,128)} %bitcast.7, ...), custom_call_target="tpu_custom_call" | custom-call | tf_op jit(solution)/shard_map/pallas_call | solution.py:991
  107.2 2.3 %copy.22 = bf16[512,1024]{1,0:T(8,128)(2,1)} copy(bf16[512,1024]{1,0:T(8,128)(2,1)} %get-tuple-element.4) | data formatting | bytes 2097152
  109.5 1.7 %copy.23 = bf16[160,1024]{1,0:T(8,128)(2,1)} copy(bf16[160,1024]{1,0:T(8,128)(2,1)} %get-tuple-element.5) | data formatting | bytes 655360

commit v2 on v1

--- a/solution.py
+++ b/solution.py
@@ -200,13 +200,13 @@
     q_hbm,
     k_hbm,
     v_hbm,
-    qgain_ref,
-    kgain_ref,
-    sink_ref,
+    qgain_hbm,
+    kgain_hbm,
+    sink_hbm,
     x_hbm,
-    gain_ref,
-    ids_ref,
-    rw_ref,
+    gain_hbm,
+    ids_hbm,
+    rw_hbm,
     gate_hbm,
     up_hbm,
     down_hbm,
@@ -233,6 +233,12 @@
     cos_ref,
     sin_ref,
     wbuf,
+    qgain_ref,
+    kgain_ref,
+    sink_ref,
+    gain_ref,
+    ids_ref,
+    rw_ref,
     scaled,
     factor,
     hid,
@@ -302,15 +308,19 @@
         return r
 
     order = (z, by_z(1, 2, 1, 2), by_z(3, 3, 0, 0), by_z(2, 0, 3, 1))
+    o1, o2, o3 = order[1:]
     k1, k2 = by_z(1, 2, 1, 2), by_z(2, 0, 3, 1)
     k3, k4 = by_z(1, 0, 3, 2), by_z(3, 3, 0, 0)
     k5, k6 = by_z(3, 2, 1, 0), by_z(2, 3, 0, 1)
 
-    def at_step(s):
-        r = order[0]
-        for i in range(1, nz):
-            r = jnp.where(s == i, order[i], r)
+    def table(s, values):
+        r = jnp.int32(values[0])
+        for i in range(1, len(values)):
+            r = jnp.where(s == i, values[i], r)
         return r
+
+    def by_kind(end, mid):
+        return jnp.where(is_end, end, mid)
 
     def rc(src, dst, s_sem, r_sem, dev):
         return pltpu.make_async_remote_copy(
@@ -333,6 +343,12 @@
         (sup_hbm, sup),
         (down_hbm.at[0], down),
         (sdown_hbm, sdown),
+        (ids_hbm, ids_ref),
+        (rw_hbm, rw_ref),
+        (qgain_hbm, qgain_ref),
+        (kgain_hbm, kgain_ref),
+        (sink_hbm, sink_ref),
+        (gain_hbm, gain_ref),
     ]
     copies = [pltpu.make_async_copy(a, b, lsem.at[i]) for i, (a, b) in enumerate(loads)]
 
@@ -341,8 +357,9 @@
         pl.semaphore_signal(barrier, inc=1, device_id=((e + d) % ep, t), device_id_type=MESH)
     for d in range(1, tp):
         pl.semaphore_signal(barrier, inc=1, device_id=(e, (t + d) % tp), device_id_type=MESH)
-    for cp in copies:
-        cp.start()
+    big = (4, 5, 6, 7, 8, 9)
+    for i in (0, 10, 11, 1, 12, 2, 3, 13, 14, 15) + big:
+        copies[i].start()
 
     quarter = HEAD_DIM // 4
     half_head = HEAD_DIM // 2
@@ -368,16 +385,14 @@
         cos_ref[rows, :] = jnp.where(lane64 < half_head, row_cos[g : g + 1, :], col_cos)
         sin_ref[rows, :] = jnp.where(lane64 < half_head, row_sin[g : g + 1, :], col_sin) * sign
 
-    padded_tok = wbuf.shape[2]
-    expert = lax.broadcasted_iota(jnp.int32, (tok, LANES), 1)
-    by_token = jnp.zeros((tok, LANES), F32)
+    copies[10].wait()
+    copies[11].wait()
+    expert = lax.broadcasted_iota(jnp.int32, (ep, tok), 0)
+    by_token = jnp.zeros((ep, tok), F32)
     for k in range(TOP_K):
-        by_token += jnp.where(ids_ref[:, k : k + 1] == expert, rw_ref[:, k : k + 1], 0.0)
-    if padded_tok > tok:
-        by_token = jnp.concatenate(
-            [by_token, jnp.zeros((padded_tok - tok, LANES), F32)], axis=0
-        )
-    wbuf[e] = by_token.T[:ep, :]
+        by_token += jnp.where(ids_ref[k : k + 1, :] == expert, rw_ref[k : k + 1, :], 0.0)
+    wbuf[e] = jnp.zeros(wbuf.shape[1:], F32)
+    wbuf[e, :, :tok] = by_token
 
     pl.semaphore_wait(barrier, ep + tp - 2)
 
@@ -505,7 +520,7 @@
     p_copy(z, t).start()
     for d in range(1, ep):
         w_copy(d).start()
-    for i in (1, 2, 3):
+    for i in (1, 2, 3, 12, 13, 14, 15):
         copies[i].wait()
 
     @pl.when(c == 0)
@@ -529,7 +544,7 @@
         kraw[end, :] = jnp.zeros((WINDOW, kv_heads * HEAD_DIM), BF16)
         vbuf[end, :] = jnp.zeros((WINDOW, kv_heads * HEAD_DIM), BF16)
 
-    trows = 64
+    trows = WINDOW
     lane = lax.broadcasted_iota(jnp.int32, (trows, LANES), 1)
     leading = (lane % half_head) < quarter
 
@@ -548,8 +563,8 @@
     def turn_rows(src, dst, count, head_gain, lo, hi, shift):
         def body(i, carry):
             rows = pl.ds(pl.multiple_of(i * trows, trows), trows)
-            table = pl.ds(pl.multiple_of(i * trows + shift, trows), trows)
-            cos, sin = cos_ref[table, :], sin_ref[table, :]
+            turned = pl.ds(pl.multiple_of(i * trows + shift, trows), trows)
+            cos, sin = cos_ref[turned, :], sin_ref[turned, :]
             for h in range(count):
                 cols = slice(h * HEAD_DIM, (h + 1) * HEAD_DIM)
                 dst[rows, cols] = turn(src[rows, cols], head_gain, cos, sin)
@@ -656,9 +671,9 @@
 
     tile = min(256, units)
 
-    def project_pair(zi):
+    def scale_rows(zi, row):
         def scale(i, carry):
-            rows = pl.ds(pl.multiple_of(i * chunk, chunk), chunk)
+            rows = pl.ds(pl.multiple_of(row + i * chunk, chunk), chunk)
             squares = jnp.zeros((chunk, 1), F32)
             for ti in range(tp):
                 v = xbuf[zi, ti, rows, :].astype(F32)
@@ -669,8 +684,9 @@
             factor[rows, :] = jnp.broadcast_to(f, (chunk, LANES))
             return carry
 
-        lax.fori_loop(0, 2 * tok // chunk, scale, 0)
-
+        lax.fori_loop(0, tok // chunk, scale, 0)
+
+    def project_pair(zi):
         def columns_of(n, carry):
             cols = pl.ds(pl.multiple_of(n * tile, tile), tile)
             g = jnp.dot(scaled[...], gate[:, cols], preferred_element_type=F32)
@@ -700,6 +716,12 @@
     ctile = min(256, columns)
     chalf = columns // 2
     per_half = chalf // ctile
+
+    def combine(zi):
+        for n in range(2):
+            pp_copy(zi, n).wait_recv()
+            qtx[zi, n] = (pbuf[zi, n, c].astype(F32) + prx[zi, n].astype(F32)).astype(BF16)
+            qq_copy(zi, n).start()
 
     def down_pair(zi):
         picked = [picks(zi * 2 + ci) for ci in range(2)]
@@ -730,20 +752,61 @@
             def _():
                 pp_copy(zi, part).start()
 
+            @pl.when((n == per_half - 1) & (zi == z))
+            def _():
+                combine(o1)
+
             return carry
 
         lax.fori_loop(0, columns // ctile, columns_of, 0)
 
-    qorder = (1, 2, 0, 3)
+    def send_h(zi):
+        for which, piece in ((0, 0), (1, 1), (0, 1), (1, 0)):
+            h_copy(zi, which, piece).start()
+
+    def forward_h(zi):
+        h_landed(zi, 0, 0).wait_recv()
+        g_copy(zi, 1).start()
+        h_landed(zi, 1, 1).wait_recv()
+        g_copy(zi, 0).start()
+
+    def shared_down():
+        for d in range(1, tp):
+            s_landed((t + d) % tp).wait_recv()
+        for n in range(2):
+            pp_copy(z, n).wait_recv()
+        for n in range(columns // ctile):
+            cols = slice(n * ctile, (n + 1) * ctile)
+            put = slice(n % per_half * ctile, (n % per_half + 1) * ctile)
+            part = n // per_half
+            acc = pbuf[z, part, c, :, put].astype(F32) + prx[z, part, :, put].astype(F32)
+            for ti in range(tp):
+                acc += jnp.dot(
+                    shbuf[ti],
+                    sdown[ti * sunits : (ti + 1) * sunits, cols],
+                    preferred_element_type=F32,
+                )
+            base[:, cols] = acc
+
+    none = -1
+    a_end, a_mid = (1, 2, 0, 3, none, none, none, none), (1, 2, none, 0, none, none, 3, none)
+    p_end = (order[0], o1, none, o2, o3, none, none, none)
+    p_mid = (order[0], o1, o3, o2, none, none, none, none)
+    d_end = (none, none, none, none, o1, order[0], o2, o3)
+    d_mid = (none, none, none, o1, order[0], o2, o3, none)
 
     def step(s, carry):
-        zi = at_step(s)
+        qb = by_kind(table(s, a_end), table(s, a_mid))
+        zi = by_kind(table(s, p_end), table(s, p_mid))
+        zq = by_kind(table(s, d_end), table(s, d_mid))
+
+        @pl.when((s == 1) & is_end)
+        def _():
+            take_t(k2)
 
         @pl.when(s == 1)
         def _():
-            @pl.when(is_end)
-            def _():
-                take_t(k2)
+            take_xy(o1)
 
         @pl.when(s == 2)
         def _():
@@ -752,6 +815,7 @@
                 wait_d(k6)
                 send_d(k6)
                 send_d(k5)
+                take_xy(o3)
 
             @pl.when(e > 0)
             def _():
@@ -767,125 +831,121 @@
             last = (nq + 1) * per_window
             turn_rows(kraw, kbuf, kv_heads, kgain_ref[...], last, last + per_window, 0)
 
-        @pl.when((s == 1) | (s == 3))
-        def _():
-            take_xy(zi)
-
-        @pl.when(s < nz)
-        def _():
-            qb = qorder[0]
-            for i in range(1, nz):
-                qb = jnp.where(s == i, qorder[i], qb)
+        @pl.when(qb >= 0)
+        def _():
             attend(qb)
             att_copy(qb).start()
 
-            @pl.when(s == 0)
+        @pl.when(s == 0)
+        def _():
+            for piece, which in ((1, 0), (0, 1)):
+                xy_landed(z, which, piece, piece * half, half).wait_recv()
+                p_copy(z, (xn, yn)[which]).start()
+            for which in range(2):
+                diagonal_landed(which).wait_recv()
+            p_copy(z, dn).start()
+            send_d(z)
+
+            @pl.when((c == 1) & (e < ep - 1))
             def _():
-                for piece, which in ((1, 0), (0, 1)):
-                    xy_landed(z, which, piece, piece * half, half).wait_recv()
-                    p_copy(z, (xn, yn)[which]).start()
-                for which in range(2):
-                    diagonal_landed(which).wait_recv()
-                p_copy(z, dn).start()
-                send_d(z)
-
-                @pl.when((c == 1) & (e < ep - 1))
-                def _():
-                    for h in halo_up:
-                        h.start()
-
-                @pl.when((c == 0) & (e > 0))
-                def _():
-                    for h in halo_down:
-                        h.start()
-
-                for d in range(1, ep):
-                    w_landed((e + d) % ep).wait_recv()
-                for cp in copies[4:]:
-                    cp.wait()
-
-            @pl.when(s == 1)
+                for h in halo_up:
+                    h.start()
+
+            @pl.when((c == 0) & (e > 0))
             def _():
-                wait_d(k3)
-                send_d(k3)
-
-                @pl.when(is_mid)
-                def _():
-                    take_t(k4)
-                    wait_d(k5)
-
-            @pl.when(s == 2)
+                for h in halo_down:
+                    h.start()
+
+            for d in range(1, ep):
+                w_landed((e + d) % ep).wait_recv()
+            for i in big:
+                copies[i].wait()
+
+        @pl.when(s == 1)
+        def _():
+            wait_d(k3)
+            send_d(k3)
+
+            @pl.when(is_mid)
             def _():
-                take_xy(zi)
-
-                @pl.when(is_end)
-                def _():
-                    wait_d(k5)
-
-            @pl.when((s == 3) & is_end)
+                take_t(k4)
+                wait_d(k5)
+
+        @pl.when((s == 3) & is_mid)
+        def _():
+            forward_h(o1)
+
+        @pl.when(s == 3)
+        def _():
+            @pl.when(is_end)
             def _():
-                wait_d(k6)
-
+                wait_d(k5)
+
+            take_xy(o2)
+
+        @pl.when((s == 4) & is_end)
+        def _():
+            wait_d(k6)
+            take_xy(o3)
+
+        @pl.when(zi >= 0)
+        def _():
+            scale_rows(zi, row_c)
             for ti in range(tp):
                 p_landed(zi, ti).wait_recv()
+            scale_rows(zi, row_o)
             project_pair(zi)
 
-            @pl.when((s == 1) & is_end)
+        @pl.when(s == 0)
+        def _():
+            send_h(z)
+            shared_up()
+            for d in range(1, tp):
+                s_copy(d).start()
+
+        @pl.when(s == 1)
+        def _():
+            @pl.when(is_end)
             def _():
                 take_t(k4)
 
-            h_copy(zi, 0, 0).start()
-            h_copy(zi, 1, 1).start()
-            h_copy(zi, 0, 1).start()
-            h_copy(zi, 1, 0).start()
-
-            @pl.when(s == 0)
+            send_h(o1)
+            forward_h(z)
+
+        @pl.when(s == 3)
+        def _():
+            @pl.when(is_end)
             def _():
-                shared_up()
-                for d in range(1, tp):
-                    s_copy(d).start()
-
-        @pl.when((s >= 1) & (s < nz + 1))
-        def _():
-            zp = at_step(s - 1)
-            h_landed(zp, 0, 0).wait_recv()
-            g_copy(zp, 1).start()
-            h_landed(zp, 1, 1).wait_recv()
-            g_copy(zp, 0).start()
-
-        @pl.when((s >= 3) & (s < nz + 3))
-        def _():
-            zq = at_step(s - 3)
+                forward_h(o1)
+
+            send_h(o2)
+
+        @pl.when(s == 4)
+        def _():
+            forward_h(o2)
+            send_h(o3)
+
+        @pl.when(zq >= 0)
+        def _():
             h_landed(zq, 0, 1).wait_recv()
             h_landed(zq, 1, 0).wait_recv()
             g_landed(zq, 0).wait_recv()
             g_landed(zq, 1).wait_recv()
             down_pair(zq)
-            for n in range(2):
-                pp_copy(zq, n).wait_recv()
-                qtx[zq, n] = (pbuf[zq, n, c].astype(F32) + prx[zq, n].astype(F32)).astype(BF16)
-
-                @pl.when(s > 3)
-                def _():
-                    qq_copy(zq, n).start()
+
+        @pl.when(zq == o2)
+        def _():
+            combine(o2)
+            forward_h(o3)
+            shared_down()
+
+        @pl.when(zq == o3)
+        def _():
+            combine(o3)
 
         return carry
 
-    lax.fori_loop(0, nz + 3, step, 0)
-
-    for d in range(1, tp):
-        s_landed((t + d) % tp).wait_recv()
-    for n in range(columns // ctile):
-        cols = slice(n * ctile, (n + 1) * ctile)
-        put = slice(n % per_half * ctile, (n % per_half + 1) * ctile)
-        acc = qtx[z, n // per_half, :, put].astype(F32)
-        for ti in range(tp):
-            acc += jnp.dot(
-                shbuf[ti],
-                sdown[ti * sunits : (ti + 1) * sunits, cols],
-                preferred_element_type=F32,
-            )
-        base[:, cols] = acc
+    lax.fori_loop(0, nz + 4, step, 0)
 
     outs = []
     for n in range(2):
@@ -981,7 +1041,6 @@
     padded_tok = (tok + LANES - 1) // LANES * LANES
     nq = tok_a // WINDOW
 
-    vm = pl.BlockSpec(memory_space=pltpu.VMEM)
     hb = pl.BlockSpec(memory_space=pl.ANY)
     dma = pltpu.SemaphoreType.DMA
     slots = 2 * cap
@@ -994,7 +1053,7 @@
             jax.ShapeDtypeStruct((tok_a, qw), BF16),
             jax.ShapeDtypeStruct((tok, columns), BF16),
         ),
-        in_specs=[hb, hb, hb, vm, vm, vm, hb, vm, vm, vm, hb, hb, hb, hb, hb, hb],
+        in_specs=[hb] * 16,
         out_specs=(hb, hb),
         scratch_shapes=[
             pltpu.VMEM((nz, tp, 2 * tok, width), BF16),
@@ -1015,6 +1074,12 @@
             pltpu.VMEM((extent, LANES), F32),
             pltpu.VMEM((extent, LANES), F32),
             pltpu.VMEM((ep, ep, padded_tok), F32),
+            pltpu.VMEM((1, HEAD_DIM), F32),
+            pltpu.VMEM((1, HEAD_DIM), F32),
+            pltpu.VMEM((1, heads), F32),
+            pltpu.VMEM((1, full), F32),
+            pltpu.VMEM((TOP_K, tok), jnp.int32),
+            pltpu.VMEM((TOP_K, tok), F32),
             pltpu.VMEM((2 * tok, full), BF16),
             pltpu.VMEM((2 * tok, LANES), F32),
             pltpu.VMEM((2 * tok, units), BF16),
@@ -1024,7 +1089,7 @@
             pltpu.VMEM((nz, 2, tok, columns // 2), BF16),
             pltpu.VMEM((nz, 2, tok, columns // 2), BF16),
             pltpu.VMEM((nz, 2, tok, columns // 2), BF16),
-            dma((10,)),
+            dma((16,)),
             dma((nq,)),
             dma((2,)),
             dma((nz, 2)),
@@ -1042,25 +1107,30 @@
         + [dma((4,))] * 2
         + two * 2,
         compiler_params=pltpu.CompilerParams(
-            collective_id=0, has_side_effects=True, vmem_limit_bytes=60 * 1024 * 1024
+            collective_id=0, has_side_effects=True, vmem_limit_bytes=50 * 1024 * 1024
         ),
     )(
-        query_vectors,
-        key_vectors,
-        value_vectors,
-        query_gain[None, :],
-        key_gain[None, :],
-        sink_logits[None, :],
-        moe_rows,
-        norm_gain[None, :],
-        expert_ids,
-        route_weights,
-        expert_gate,
-        expert_up,
-        expert_down,
-        shared_gate,
-        shared_up,
-        shared_down,
+        *(
+            pltpu.with_memory_space_constraint(x, pltpu.HBM)
+            for x in (
+                query_vectors,
+                key_vectors,
+                value_vectors,
+                query_gain[None, :],
+                key_gain[None, :],
+                sink_logits[None, :],
+                moe_rows,
+                norm_gain[None, :],
+                expert_ids.T,
+                route_weights.T,
+                expert_gate,
+                expert_up,
+                expert_down,
+                shared_gate,
+                shared_up,
+                shared_down,
+            )
+        )
     )
 
 

time: 111 us -> 98.3 us (0.89)
  Pallas kernels: 104 us -> 95.8 us
  local copies, waits for them, and re-layouts: 6.85 us -> 1.7 us
    pallas_call x1, Pallas kernels: 104 us -> 95.8 us  [fast_shards(): pl.pallas_call(functools.partial(line_kernel, sizes), out_shape=(jax.Shap...]
    unnamed x4 -> x2, local copies, waits for them, and re-layouts: 6.85 us -> 1.7 us
where the time goes in v2:
time: 98.3 us; the launch traced here: 98.1 us
  Pallas kernels  95.8 us (97%)
  local copies, waits for them, and re-layouts  1.7 us (2%)
    pallas_call x1, Pallas kernels, fast_shards(): pl.pallas_call(functools.partial(line_kernel, sizes), out_shape=(jax.Shap...  95.8 us

profile of v2, /device:TPU:0, one launch (start us, length us, event | category | flops | bytes accessed | tf_op | source)
XLA Modules:
  0.0 98.1 jit_solution(18403904055034880239)
XLA Ops:
  0.6 95.8 %shard_map.167 = (bf16[512,1024]{1,0:T(8,128)(2,1)S(1)}, bf16[160,1024]{1,0:T(8,128)(2,1)S(1)}) custom-call(bf16[512,1024]{1,0:T(8,128)(2,1)} %q_hbm.1, bf16[512,512]{1,0:T(8,128)(2,1)} %k_hbm.1, bf16[512,512]{1,0:T(8,128)(2,1)} %v_hbm.1, f32[1,128]{1,0:T(1,128)} %bitcast.9, f32[1,128]{1,0:T(1,128)} %bitcast.10, f32[1,8]{1,0:T(1,128)} %bitcast.11, ...), custom_call_target="tpu_custom_call" | custom-call | tf_op jit(solution)/shard_map/pallas_call | solution.py:1050
  96.4 1.0 copy.20
  97.4 0.7 copy.21

commit v3 on v2

--- a/solution.py
+++ b/solution.py
@@ -255,6 +255,8 @@
     ztr,
     zds,
     zdr,
+    zxs,
+    zxr,
     xs,
     xr,
     ys,
@@ -425,6 +427,15 @@
     def send_d(zi):
         along(zi, lambda way: zd_copy(zi, way).start())
 
+    def zx_copy(which):
+        u = unit(z, (xn, yn)[which], row_c)
+        dev = jnp.where(z == 0, up_z, down_z)
+        return rc(u, u, zxs.at[which], zxr.at[which], (dev, t))
+
+    def zx_landed(which):
+        u = unit(o3, (xn, yn)[which], row_c)
+        return rc(u, u, zxs.at[which], zxr.at[which], (e, xn))
+
     def xy_copy(zi, which, piece, first, count):
         u = unit(zi, t, row_c, first, count)
         sems = (xs, xr) if which == 0 else (ys, yr)
@@ -583,11 +594,12 @@
 
     turn_rows(kraw, kbuf, kv_heads, kgain_ref[...], per_window, (nq + 1) * per_window, 0)
 
-    def take_t(zi):
+    def take_t(zi, spread=True):
         u = unit(zi, t, row_c)
         rc(u, u, zts.at[zi, 0], ztr.at[zi], (e, xn)).wait_recv()
-        xy_copy(zi, 0, 0, 0, tok).start()
-        xy_copy(zi, 1, 0, 0, tok).start()
+        if spread:
+            xy_copy(zi, 0, 0, 0, tok).start()
+            xy_copy(zi, 1, 0, 0, tok).start()
         send_t(zi)
         p_copy(zi, t).start()
 
@@ -606,7 +618,7 @@
 
     @pl.when(is_mid)
     def _():
-        take_t(k2)
+        take_t(k2, spread=False)
 
     span = 3 * WINDOW
     near = lax.broadcasted_iota(jnp.int32, (WINDOW, WINDOW), 1)
@@ -663,6 +675,16 @@
         hot = jnp.where((slot == rank) & (named > 0.0), 1.0, 0.0)
         return hot, jnp.sum(hot * weight, axis=1, keepdims=True)
 
+    def send_h(zi):
+        for which, piece in ((0, 0), (1, 1), (0, 1), (1, 0)):
+            h_copy(zi, which, piece).start()
+
+    def forward_h(zi):
+        h_landed(zi, 0, 0).wait_recv()
+        g_copy(zi, 1).start()
+        h_landed(zi, 1, 1).wait_recv()
+        g_copy(zi, 0).start()
+
     chunk = 32
 
     def silu_pair(g, u, f):
@@ -688,6 +710,25 @@
 
     def project_pair(zi):
         def columns_of(n, carry):
+            @pl.when((n == 1) & is_end & (zi == z))
+            def _():
+                take_t(k2)
+
+            @pl.when((n == 1) & is_end & (zi == o2))
+            def _():
+                forward_h(o1)
+
+            @pl.when((n == 1) & is_end & (zi == o3))
+            def _():
+                forward_h(o2)
+
+            @pl.when((n == 1) & is_mid & (zi == o2))
+            def _():
+                forward_h(o1)
+                for which in range(2):
+                    zx_landed(which).wait_recv()
+                    p_copy(o3, (xn, yn)[which]).start()
+
             cols = pl.ds(pl.multiple_of(n * tile, tile), tile)
             g = jnp.dot(scaled[...], gate[:, cols], preferred_element_type=F32)
             u = jnp.dot(scaled[...], up[:, cols], preferred_element_type=F32)
@@ -717,11 +758,10 @@
     chalf = columns // 2
     per_half = chalf // ctile
 
-    def combine(zi):
-        for n in range(2):
-            pp_copy(zi, n).wait_recv()
-            qtx[zi, n] = (pbuf[zi, n, c].astype(F32) + prx[zi, n].astype(F32)).astype(BF16)
-            qq_copy(zi, n).start()
+    def combine(zi, n):
+        pp_copy(zi, n).wait_recv()
+        qtx[zi, n] = (pbuf[zi, n, c].astype(F32) + prx[zi, n].astype(F32)).astype(BF16)
+        qq_copy(zi, n).start()
 
     def down_pair(zi):
         picked = [picks(zi * 2 + ci) for ci in range(2)]
@@ -752,23 +792,18 @@
             def _():
                 pp_copy(zi, part).start()
 
-            @pl.when((n == per_half - 1) & (zi == z))
-            def _():
-                combine(o1)
+            @pl.when((n == per_half - 1) & (zi == by_kind(o2, z)))
+            def _():
+                combine(o1, 0)
+                combine(o1, 1)
+
+            @pl.when((n == per_half) & (zi == o3))
+            def _():
+                combine(o3, 0)
 
             return carry
 
         lax.fori_loop(0, columns // ctile, columns_of, 0)
-
-    def send_h(zi):
-        for which, piece in ((0, 0), (1, 1), (0, 1), (1, 0)):
-            h_copy(zi, which, piece).start()
-
-    def forward_h(zi):
-        h_landed(zi, 0, 0).wait_recv()
-        g_copy(zi, 1).start()
-        h_landed(zi, 1, 1).wait_recv()
-        g_copy(zi, 0).start()
 
     def shared_down():
         for d in range(1, tp):
@@ -789,10 +824,10 @@
             base[:, cols] = acc
 
     none = -1
-    a_end, a_mid = (1, 2, 0, 3, none, none, none, none), (1, 2, none, 0, none, none, 3, none)
+    a_end, a_mid = (1, 2, 0, none, none, none, 3, none), (1, 2, none, none, none, none, 0, 3)
     p_end = (order[0], o1, none, o2, o3, none, none, none)
-    p_mid = (order[0], o1, o3, o2, none, none, none, none)
-    d_end = (none, none, none, none, o1, order[0], o2, o3)
+    p_mid = (order[0], o1, o2, o3, none, none, none, none)
+    d_end = (none, none, order[0], none, o1, o2, o3, none)
     d_mid = (none, none, none, o1, order[0], o2, o3, none)
 
     def step(s, carry):
@@ -800,23 +835,23 @@
         zi = by_kind(table(s, p_end), table(s, p_mid))
         zq = by_kind(table(s, d_end), table(s, d_mid))
 
-        @pl.when((s == 1) & is_end)
-        def _():
-            take_t(k2)
-
         @pl.when(s == 1)
         def _():
+            @pl.when(is_mid)
+            def _():
+                take_t(k4)
+
             take_xy(o1)
 
-        @pl.when(s == 2)
-        def _():
-            @pl.when(is_mid)
-            def _():
-                wait_d(k6)
-                send_d(k6)
-                send_d(k5)
-                take_xy(o3)
-
+        @pl.when((s == 2) & is_mid)
+        def _():
+            wait_d(k6)
+            send_d(k6)
+            send_d(k5)
+            take_xy(o2)
+
+        @pl.when(s == by_kind(2, 6))
+        def _():
             @pl.when(e > 0)
             def _():
                 for h in halo_up:
@@ -830,6 +865,10 @@
             turn_rows(kraw, kbuf, kv_heads, kgain_ref[...], 0, per_window, 0)
             last = (nq + 1) * per_window
             turn_rows(kraw, kbuf, kv_heads, kgain_ref[...], last, last + per_window, 0)
+
+        @pl.when((s == 3) & is_end)
+        def _():
+            take_xy(o3)
 
         @pl.when(qb >= 0)
         def _():
@@ -856,6 +895,11 @@
                 for h in halo_down:
                     h.start()
 
+            @pl.when(is_end)
+            def _():
+                zx_copy(0).start()
+                zx_copy(1).start()
+
             for d in range(1, ep):
                 w_landed((e + d) % ep).wait_recv()
             for i in big:
@@ -868,29 +912,21 @@
 
             @pl.when(is_mid)
             def _():
-                take_t(k4)
                 wait_d(k5)
 
-        @pl.when((s == 3) & is_mid)
-        def _():
-            forward_h(o1)
-
-        @pl.when(s == 3)
-        def _():
-            @pl.when(is_end)
-            def _():
-                wait_d(k5)
-
+        @pl.when((s == 3) & is_end)
+        def _():
+            wait_d(k5)
             take_xy(o2)
 
         @pl.when((s == 4) & is_end)
         def _():
             wait_d(k6)
-            take_xy(o3)
 
         @pl.when(zi >= 0)
         def _():
             scale_rows(zi, row_c)
+
             for ti in range(tp):
                 p_landed(zi, ti).wait_recv()
             scale_rows(zi, row_o)
@@ -905,24 +941,24 @@
 
         @pl.when(s == 1)
         def _():
+            forward_h(z)
+
             @pl.when(is_end)
             def _():
                 take_t(k4)
 
             send_h(o1)
-            forward_h(z)
-
-        @pl.when(s == 3)
-        def _():
-            @pl.when(is_end)
-            def _():
-                forward_h(o1)
-
+
+        @pl.when(s == by_kind(3, 2))
+        def _():
             send_h(o2)
 
-        @pl.when(s == 4)
+        @pl.when((s == 3) & is_mid)
         def _():
             forward_h(o2)
+
+        @pl.when(s == by_kind(4, 3))
+        def _():
             send_h(o3)
 
         @pl.when(zq >= 0)
@@ -935,17 +971,65 @@
 
         @pl.when(zq == o2)
         def _():
-            combine(o2)
             forward_h(o3)
+            combine(o2, 0)
+            combine(o2, 1)
             shared_down()
 
         @pl.when(zq == o3)
         def _():
-            combine(o3)
+            combine(o3, 1)
 
         return carry
 
     lax.fori_loop(0, nz + 4, step, 0)
+
+    def drain(zi, carry):
+        along(zi, lambda way: zt_copy(zi, way).wait_send())
+        along(zi, lambda way: zd_copy(zi, way).wait_send())
+        for which in range(2):
+            g_copy(zi, which).wait_send()
+            for piece in range(2):
+                h_copy(zi, which, piece).wait_send()
+        for n in range(2):
+            pp_copy(zi, n).wait_send()
+        for ti in range(tp):
+            p_copy(zi, ti).wait_send()
+
+        @pl.when((zi != z) & (is_end | (zi != o3)))
+        def _():
+            for which in range(2):
+                xy_copy(zi, which, 0, 0, tok).wait_send()
+
+        return carry
+
+    lax.fori_loop(0, nz, drain, 0)
+    for which in range(2):
+        diagonal(which).wait_send()
+        for piece in range(2):
+            xy_copy(z, which, piece, piece * half, half).wait_send()
+    for d in range(1, tp):
+        s_copy(d).wait_send()
+    for d in range(1, ep):
+        w_copy(d).wait_send()
+
+    @pl.when(e < ep - 1)
+    def _():
+        for h in halo_up:
+            h.wait_send()
+
+    @pl.when(e > 0)
+    def _():
+        for h in halo_down:
+            h.wait_send()
+
+    @pl.when(is_end)
+    def _():
+        for which in range(2):
+            zx_copy(which).wait_send()
+
+    for qb in range(nq):
+        att_copy(qb).wait()
 
     outs = []
     for n in range(2):
@@ -959,49 +1043,9 @@
         outs.append(pltpu.make_async_copy(obuf.at[n], out_hbm.at[:, cols], osem.at[n]))
         outs[-1].start()
 
-    def drain(zi, carry):
-        along(zi, lambda way: zt_copy(zi, way).wait_send())
-        along(zi, lambda way: zd_copy(zi, way).wait_send())
-        for which in range(2):
-            g_copy(zi, which).wait_send()
-            for piece in range(2):
-                h_copy(zi, which, piece).wait_send()
+    for i in range(1, nz):
         for n in range(2):
-            pp_copy(zi, n).wait_send()
-        for ti in range(tp):
-            p_copy(zi, ti).wait_send()
-
-        @pl.when(zi != z)
-        def _():
-            for which in range(2):
-                xy_copy(zi, which, 0, 0, tok).wait_send()
-            for n in range(2):
-                qq_copy(zi, n).wait_send()
-
-        return carry
-
-    lax.fori_loop(0, nz, drain, 0)
-    for which in range(2):
-        diagonal(which).wait_send()
-        for piece in range(2):
-            xy_copy(z, which, piece, piece * half, half).wait_send()
-    for d in range(1, tp):
-        s_copy(d).wait_send()
-    for d in range(1, ep):
-        w_copy(d).wait_send()
-
-    @pl.when(e < ep - 1)
-    def _():
-        for h in halo_up:
-            h.wait_send()
-
-    @pl.when(e > 0)
-    def _():
-        for h in halo_down:
-            h.wait_send()
-
-    for qb in range(nq):
-        att_copy(qb).wait()
+            qq_copy(order[i], n).wait_send()
     for cp in outs:
         cp.wait()
 
@@ -1097,6 +1141,7 @@
             dma((nz, 2)),
             dma((nz,)),
         ]
+        + [dma((2,))] * 2
         + two * 2
         + [dma((2,))] * 2
         + four

time: 98.3 us -> 94.2 us (0.958)
  Pallas kernels: 95.8 us -> 91.8 us
    pallas_call x1, Pallas kernels: 95.8 us -> 91.8 us  [fast_shards(): pl.pallas_call(functools.partial(line_kernel, sizes), out_shape=(jax.Shap...]
where the time goes in v3:
time: 94.2 us; the launch traced here: 94.1 us
  Pallas kernels  91.8 us (97%)
  local copies, waits for them, and re-layouts  1.7 us (2%)
    pallas_call x1, Pallas kernels, fast_shards(): pl.pallas_call(functools.partial(line_kernel, sizes), out_shape=(jax.Shap...  91.8 us

profile of v3, /device:TPU:0, one launch (start us, length us, event | category | flops | bytes accessed | tf_op | source)
XLA Modules:
  0.0 94.1 jit_solution(5524411830280219298)
XLA Ops:
  0.6 91.8 %shard_map.167 = (bf16[512,1024]{1,0:T(8,128)(2,1)S(1)}, bf16[160,1024]{1,0:T(8,128)(2,1)S(1)}) custom-call(bf16[512,1024]{1,0:T(8,128)(2,1)} %q_hbm.1, bf16[512,512]{1,0:T(8,128)(2,1)} %k_hbm.1, bf16[512,512]{1,0:T(8,128)(2,1)} %v_hbm.1, f32[1,128]{1,0:T(1,128)} %bitcast.9, f32[1,128]{1,0:T(1,128)} %bitcast.10, f32[1,8]{1,0:T(1,128)} %bitcast.11, ...), custom_call_target="tpu_custom_call" | custom-call | tf_op jit(solution)/shard_map/pallas_call | solution.py:1094
  92.4 1.0 %copy.20 = bf16[512,1024]{1,0:T(8,128)(2,1)} copy(bf16[512,1024]{1,0:T(8,128)(2,1)S(1)} %get-tuple-element.4) | data formatting | bytes 2097152
  93.4 0.7 copy.21

commit v4 on v3

--- a/solution.py
+++ b/solution.py
@@ -249,8 +249,6 @@
     qtx,
     qrx,
     lsem,
-    asem,
-    osem,
     zts,
     ztr,
     zds,
@@ -439,12 +437,12 @@
     def xy_copy(zi, which, piece, first, count):
         u = unit(zi, t, row_c, first, count)
         sems = (xs, xr) if which == 0 else (ys, yr)
-        return rc(u, u, sems[0].at[zi, piece], sems[1].at[zi, piece], (e, (xn, yn)[which]))
+        return rc(u, u, sems[0], sems[1].at[zi, piece], (e, (xn, yn)[which]))
 
     def xy_landed(zi, which, piece, first, count):
         u = unit(zi, (xn, yn)[which], row_c, first, count)
         sems = (xs, xr) if which == 0 else (ys, yr)
-        return rc(u, u, sems[0].at[zi, piece], sems[1].at[zi, piece], (e, (xn, yn)[which]))
+        return rc(u, u, sems[0], sems[1].at[zi, piece], (e, (xn, yn)[which]))
 
     def diagonal(which):
         source, first = ((yn, half), (xn, 0))[which]
@@ -457,49 +455,53 @@
 
     def p_copy(zi, ti):
         u = unit(zi, ti, row_c)
-        return rc(u, u, ps.at[zi, ti], pr.at[zi, ti], (partner, t))
-
-    def p_landed(zi, ti):
-        u = unit(zi, ti, row_o)
-        return rc(u, u, ps.at[zi, ti], pr.at[zi, ti], (partner, t))
+        return rc(u, u, ps, pr.at[zi], (partner, t))
+
+    def p_landed(zi):
+        u = xbuf.at[zi, :, pl.ds(row_o, tok), :]
+        return rc(u, u, ps, pr.at[zi], (partner, t))
 
     h_parts = ((0, hcut), (hcut, slots - hcut))
 
     def h_copy(zi, which, piece):
         u = hbuf.at[zi, t, pl.ds(*h_parts[piece]), :]
         sems = (hxs, hxr) if which == 0 else (hys, hyr)
-        return rc(u, u, sems[0].at[zi, piece], sems[1].at[zi, piece], (e, (xn, yn)[which]))
+        return rc(u, u, sems[0], sems[1].at[zi, piece], (e, (xn, yn)[which]))
 
     def h_landed(zi, which, piece):
         u = hbuf.at[zi, (xn, yn)[which], pl.ds(*h_parts[piece]), :]
         sems = (hxs, hxr) if which == 0 else (hys, hyr)
-        return rc(u, u, sems[0].at[zi, piece], sems[1].at[zi, piece], (e, (xn, yn)[which]))
+        return rc(u, u, sems[0], sems[1].at[zi, piece], (e, (xn, yn)[which]))
 
     def g_copy(zi, which):
         u = hbuf.at[zi, (yn, xn)[which], pl.ds(*h_parts[1 - which]), :]
         sems = (gxs, gxr) if which == 0 else (gys, gyr)
-        return rc(u, u, sems[0].at[zi], sems[1].at[zi], (e, (xn, yn)[which]))
+        return rc(u, u, sems[0], sems[1].at[zi], (e, (xn, yn)[which]))
 
     def g_landed(zi, which):
         u = hbuf.at[zi, dn, pl.ds(*h_parts[1 - which]), :]
         sems = (gxs, gxr) if which == 0 else (gys, gyr)
-        return rc(u, u, sems[0].at[zi], sems[1].at[zi], (e, (xn, yn)[which]))
+        return rc(u, u, sems[0], sems[1].at[zi], (e, (xn, yn)[which]))
 
     def s_copy(d):
         u = shbuf.at[t]
-        return rc(u, u, ss.at[d], sr.at[t], (e, (t + d) % tp))
-
-    def s_landed(ti):
-        u = shbuf.at[ti]
-        return rc(u, u, ss.at[0], sr.at[ti], (e, xn))
+        return rc(u, u, ss, sr, (e, (t + d) % tp))
 
     def w_copy(d):
         u = wbuf.at[e]
-        return rc(u, u, ws.at[d], wr.at[e], ((e + d) % ep, t))
-
-    def w_landed(ei):
-        u = wbuf.at[ei]
-        return rc(u, u, ws.at[0], wr.at[ei], (partner, t))
+        return rc(u, u, ws, wr, ((e + d) % ep, t))
+
+    def all_s():
+        u = shbuf.at[pl.ds(0, tp - 1)]
+        return rc(u, u, ss, sr, (e, xn))
+
+    def all_w():
+        u = wbuf.at[pl.ds(0, ep - 1)]
+        return rc(u, u, ws, wr, (partner, t))
+
+    def all_qq(n):
+        u = qrx.at[pl.ds(0, nz - 1), n]
+        return rc(u, u, qqs.at[0], qqr.at[n], (partner, t))
 
     after, before = jnp.minimum(e + 1, ep - 1), jnp.maximum(e - 1, 0)
     tail, first = pl.ds(tok_a, WINDOW), pl.ds(WINDOW, WINDOW)
@@ -514,13 +516,10 @@
     ]
 
     def pp_copy(zi, n):
-        return rc(pbuf.at[zi, n, other], prx.at[zi, n], pps.at[zi, n], ppr.at[zi, n], (partner, t))
+        return rc(pbuf.at[zi, n, other], prx.at[zi, n], pps, ppr.at[zi, n], (partner, t))
 
     def qq_copy(zi, n):
-        return rc(qtx.at[zi, n], qrx.at[z, n], qqs.at[zi, n], qqr.at[z, n], (zi * 2 + c, t))
-
-    def qq_landed(zi, n):
-        return rc(qrx.at[zi, n], qrx.at[zi, n], qqs.at[zi, n], qqr.at[zi, n], (partner, t))
+        return rc(qtx.at[zi, n], qrx.at[z, n], qqs.at[zi], qqr.at[n], (zi * 2 + c, t))
 
     copies[0].wait()
     xy_copy(z, 0, 0, 0, half).start()
@@ -656,7 +655,7 @@
 
     def att_copy(qb):
         rows = pl.ds(pl.multiple_of(qb * WINDOW, WINDOW), WINDOW)
-        return pltpu.make_async_copy(abuf.at[rows, :], att_hbm.at[rows, :], asem.at[qb])
+        return pltpu.make_async_copy(abuf.at[rows, :], att_hbm.at[rows, :], lsem.at[qb])
 
     upper = (
         lax.broadcasted_iota(jnp.int32, (tok, tok), 0)
@@ -806,8 +805,7 @@
         lax.fori_loop(0, columns // ctile, columns_of, 0)
 
     def shared_down():
-        for d in range(1, tp):
-            s_landed((t + d) % tp).wait_recv()
+        all_s().wait_recv()
         for n in range(2):
             pp_copy(z, n).wait_recv()
         for n in range(columns // ctile):
@@ -900,8 +898,7 @@
                 zx_copy(0).start()
                 zx_copy(1).start()
 
-            for d in range(1, ep):
-                w_landed((e + d) % ep).wait_recv()
+            all_w().wait_recv()
             for i in big:
                 copies[i].wait()
 
@@ -927,8 +924,7 @@
         def _():
             scale_rows(zi, row_c)
 
-            for ti in range(tp):
-                p_landed(zi, ti).wait_recv()
+            p_landed(zi).wait_recv()
             scale_rows(zi, row_o)
             project_pair(zi)
 
@@ -984,34 +980,35 @@
 
     lax.fori_loop(0, nz + 4, step, 0)
 
+    def sent(u, sem):
+        rc(u, u, sem, pr.at[0], (partner, t)).wait_send()
+
     def drain(zi, carry):
         along(zi, lambda way: zt_copy(zi, way).wait_send())
         along(zi, lambda way: zd_copy(zi, way).wait_send())
-        for which in range(2):
-            g_copy(zi, which).wait_send()
-            for piece in range(2):
-                h_copy(zi, which, piece).wait_send()
-        for n in range(2):
-            pp_copy(zi, n).wait_send()
-        for ti in range(tp):
-            p_copy(zi, ti).wait_send()
-
-        @pl.when((zi != z) & (is_end | (zi != o3)))
-        def _():
-            for which in range(2):
-                xy_copy(zi, which, 0, 0, tok).wait_send()
-
         return carry
 
     lax.fori_loop(0, nz, drain, 0)
+
+    @pl.when(is_end)
+    def _():
+        for sem in (xs, ys):
+            sent(xbuf.at[:, t, pl.ds(row_c, tok), :], sem)
+
+    @pl.when(is_mid)
+    def _():
+        for sem in (xs, ys):
+            sent(xbuf.at[pl.ds(0, nz - 1), t, pl.ds(row_c, tok), :], sem)
+
+    for which in range(2):
+        sent(hbuf.at[:, t], (hxs, hys)[which])
+        sent(hbuf.at[:, t, pl.ds(*h_parts[1 - which]), :], (gxs, gys)[which])
+    sent(xbuf.at[:, :, pl.ds(row_c, tok), :], ps)
+    sent(pbuf.at[:, :, other], pps)
+    all_s().wait_send()
+    all_w().wait_send()
     for which in range(2):
         diagonal(which).wait_send()
-        for piece in range(2):
-            xy_copy(z, which, piece, piece * half, half).wait_send()
-    for d in range(1, tp):
-        s_copy(d).wait_send()
-    for d in range(1, ep):
-        w_copy(d).wait_send()
 
     @pl.when(e < ep - 1)
     def _():
@@ -1033,19 +1030,17 @@
 
     outs = []
     for n in range(2):
-        for i in range(1, nz):
-            qq_landed(order[i], n).wait_recv()
+        all_qq(n).wait_recv()
         cols = slice(n * chalf, (n + 1) * chalf)
         acc = base[:, cols]
         for i in range(1, nz):
             acc += qrx[order[i], n].astype(F32)
         obuf[n] = acc.astype(BF16)
-        outs.append(pltpu.make_async_copy(obuf.at[n], out_hbm.at[:, cols], osem.at[n]))
+        outs.append(pltpu.make_async_copy(obuf.at[n], out_hbm.at[:, cols], lsem.at[4 + n]))
         outs[-1].start()
 
     for i in range(1, nz):
-        for n in range(2):
-            qq_copy(order[i], n).wait_send()
+        sent(qtx.at[order[i]], qqs.at[order[i]])
     for cp in outs:
         cp.wait()
 
@@ -1090,7 +1085,6 @@
     slots = 2 * cap
     kvw = kv_heads * HEAD_DIM
     qw = heads * HEAD_DIM
-    one, two, four = [dma((nz,))] * 2, [dma((nz, 2))] * 2, [dma((nz, tp))] * 2
     return pl.pallas_call(
         functools.partial(line_kernel, sizes),
         out_shape=(
@@ -1134,23 +1128,20 @@
             pltpu.VMEM((nz, 2, tok, columns // 2), BF16),
             pltpu.VMEM((nz, 2, tok, columns // 2), BF16),
             dma((16,)),
-            dma((nq,)),
-            dma((2,)),
             dma((nz, 2)),
             dma((nz,)),
             dma((nz, 2)),
             dma((nz,)),
         ]
         + [dma((2,))] * 2
-        + two * 2
+        + [dma, dma((nz, 2))] * 2
         + [dma((2,))] * 2
-        + four
-        + two * 2
-        + one * 2
-        + [dma((tp,))] * 2
-        + [dma((ep,))] * 2
+        + [dma, dma((nz,))]
+        + [dma, dma((nz, 2))] * 2
+        + [dma, dma((nz,))] * 2
+        + [dma] * 4
         + [dma((4,))] * 2
-        + two * 2,
+        + [dma, dma((nz, 2)), dma((nz,)), dma((2,))],
         compiler_params=pltpu.CompilerParams(
             collective_id=0, has_side_effects=True, vmem_limit_bytes=50 * 1024 * 1024
         ),

time: 94.2 us -> 93.3 us (level)
  Pallas kernels: 91.8 us -> 90.8 us
    pallas_call x1, Pallas kernels: 91.8 us -> 90.8 us  [fast_shards(): pl.pallas_call(functools.partial(line_kernel, sizes), out_shape=(jax.Shap...]
where the time goes in v4:
time: 93.3 us; the launch traced here: 93.1 us
  Pallas kernels  90.8 us (97%)
  local copies, waits for them, and re-layouts  1.7 us (2%)
    pallas_call x1, Pallas kernels, fast_shards(): pl.pallas_call(functools.partial(line_kernel, sizes), out_shape=(jax.Shap...  90.8 us

profile of v4, /device:TPU:0, one launch (start us, length us, event | category | flops | bytes accessed | tf_op | source)
XLA Modules:
  0.0 93.1 jit_solution(16500228720831569261)
XLA Ops:
  0.6 90.8 %shard_map.167 = (bf16[512,1024]{1,0:T(8,128)(2,1)S(1)}, bf16[160,1024]{1,0:T(8,128)(2,1)S(1)}) custom-call(bf16[512,1024]{1,0:T(8,128)(2,1)} %q_hbm.1, bf16[512,512]{1,0:T(8,128)(2,1)} %k_hbm.1, bf16[512,512]{1,0:T(8,128)(2,1)} %v_hbm.1, f32[1,128]{1,0:T(1,128)} %bitcast.9, f32[1,128]{1,0:T(1,128)} %bitcast.10, f32[1,8]{1,0:T(1,128)} %bitcast.11, ...), custom_call_target="tpu_custom_call" | custom-call | tf_op jit(solution)/shard_map/pallas_call | solution.py:1088
  91.5 1.0 %copy.20 = bf16[512,1024]{1,0:T(8,128)(2,1)} copy(bf16[512,1024]{1,0:T(8,128)(2,1)S(1)} %get-tuple-element.4) | data formatting | bytes 2097152
  92.4 0.7 copy.21

commit v5 on v4

--- a/solution.py
+++ b/solution.py
@@ -822,11 +822,11 @@
             base[:, cols] = acc
 
     none = -1
-    a_end, a_mid = (1, 2, 0, none, none, none, 3, none), (1, 2, none, none, none, none, 0, 3)
-    p_end = (order[0], o1, none, o2, o3, none, none, none)
-    p_mid = (order[0], o1, o2, o3, none, none, none, none)
-    d_end = (none, none, order[0], none, o1, o2, o3, none)
-    d_mid = (none, none, none, o1, order[0], o2, o3, none)
+    a_end, a_mid = (1, 2, 0, none, none, none, none, 3, none), (1, 2, none, none, none, none, none, 0, 3)
+    p_end = (order[0], o1, none, o2, o3, none, none, none, none)
+    p_mid = (order[0], o1, o2, o3, none, none, none, none, none)
+    d_end = (none, none, order[0], none, o1, o2, o3, none, none)
+    d_mid = (none, none, none, o1, order[0], o2, o3, none, none)
 
     def step(s, carry):
         qb = by_kind(table(s, a_end), table(s, a_mid))
@@ -848,7 +848,7 @@
             send_d(k5)
             take_xy(o2)
 
-        @pl.when(s == by_kind(2, 6))
+        @pl.when(s == by_kind(2, 7))
         def _():
             @pl.when(e > 0)
             def _():
@@ -978,7 +978,7 @@
 
         return carry
 
-    lax.fori_loop(0, nz + 4, step, 0)
+    lax.fori_loop(0, nz + 5, step, 0)
 
     def sent(u, sem):
         rc(u, u, sem, pr.at[0], (partner, t)).wait_send()

time: 93.3 us -> 93.3 us (level)
  no operation moved by 1% of the time
where the time goes in v5:
time: 93.3 us; the launch traced here: 93.1 us
  Pallas kernels  90.8 us (97%)
  local copies, waits for them, and re-layouts  1.7 us (2%)
    pallas_call x1, Pallas kernels, fast_shards(): pl.pallas_call(functools.partial(line_kernel, sizes), out_shape=(jax.Shap...  90.8 us

profile of v5, /device:TPU:0, one launch (start us, length us, event | category | flops | bytes accessed | tf_op | source)
XLA Modules:
  0.0 93.1 jit_solution(8790891935052298712)
XLA Ops:
  0.6 90.8 %shard_map.167 = (bf16[512,1024]{1,0:T(8,128)(2,1)S(1)}, bf16[160,1024]{1,0:T(8,128)(2,1)S(1)}) custom-call(bf16[512,1024]{1,0:T(8,128)(2,1)} %q_hbm.1, bf16[512,512]{1,0:T(8,128)(2,1)} %k_hbm.1, bf16[512,512]{1,0:T(8,128)(2,1)} %v_hbm.1, f32[1,128]{1,0:T(1,128)} %bitcast.9, f32[1,128]{1,0:T(1,128)} %bitcast.10, f32[1,8]{1,0:T(1,128)} %bitcast.11, ...), custom_call_target="tpu_custom_call" | custom-call | tf_op jit(solution)/shard_map/pallas_call | solution.py:1088
  91.5 1.0 %copy.20 = bf16[512,1024]{1,0:T(8,128)(2,1)} copy(bf16[512,1024]{1,0:T(8,128)(2,1)S(1)} %get-tuple-element.4) | data formatting | bytes 2097152
  92.4 0.7 copy.21
